TPU v7x, 128 devices: a whole 4x4x4 slice. The times are simulated.
128 devices in a mesh: sp: 16 (over z, y), fs: 4 (over x), tp: 2 (over core).
Axes of the slice: x: 4, y: 4, z: 4, core: 2. Of those that a mesh axis runs over, the one named last changes fastest.
Arguments:
- hidden_in: bfloat16 [32768, 2048], P(('fs', 'sp'), 'tp'), parts along dimension 0, may hold values from -6 to 48
- in_gain: float32 [2048], replicated, may hold values from 0.1 to 1.9
- w_query: bfloat16 [2048, 1024], P(None, 'tp'), may hold values from -0.29972302 to 0.29972302
- w_key: bfloat16 [2048, 1024], P(None, 'tp'), may hold values from -0.29972302 to 0.29972302
- w_value: bfloat16 [2048, 1024], P(None, 'tp'), may hold values from -0.125 to 0.125
- w_gate: bfloat16 [2048, 1024], P(None, 'tp'), may hold values from -0.125 to 0.125
- w_inner: bfloat16 [2048, 1024], P(None, 'tp'), may hold values from -0.125 to 0.125
- w_bvec: bfloat16 [2048, 512], P(None, 'tp'), may hold values from -0.125 to 0.125
- w_cvec: bfloat16 [2048, 512], P(None, 'tp'), may hold values from -0.125 to 0.125
- w_step: bfloat16 [2048, 16], P(None, 'tp'), may hold values from -0.125 to 0.125
- conv_inner: bfloat16 [4, 1024], P(None, 'tp'), may hold values from -3 to 3
- conv_bvec: bfloat16 [4, 512], P(None, 'tp'), may hold values from -3 to 3
- conv_cvec: bfloat16 [4, 512], P(None, 'tp'), may hold values from -3 to 3
- a_log: float32 [16], P('tp'), may hold values from -16 to 0
- decay_add: float32 [32768, 16], P(('fs', 'sp'), 'tp'), parts along dimension 0, may hold values from -1 to 0
- lambdas: float32 [4], P('tp'), may hold values from 0.3 to 0.8
- head_gain: float32 [256], replicated, may hold values from 0.1 to 1.9
- ssm_gain: float32 [1024], P('tp'), may hold values from 0.1 to 1.9
- out_attn: bfloat16 [1024, 2048], P('tp'), may hold values from -0.125 to 0.125
- out_ssm: bfloat16 [1024, 2048], P('tp'), may hold values from -0.125 to 0.125
Outputs:
- layer_out: bfloat16 [32768, 2048], P(('fs', 'sp', 'tp')), parts along dimension 0
There are 4 independent parts, one for each index of `fs`. A program takes and returns all parts, laid end to end along the dimension named above; an argument that names none is the same for every part. Nothing has to cross between parts.
All inputs are finite; a program needn't handle non-finite values.
Results may differ from a plain program's by a relative error of at most 0.012.
The roundings to bfloat16 on the way count: a program that leaves them out, or rounds other values in their place, can miss the bound.
Values may be sent and summed in bfloat16 or wider, within the bound.
A program may use at most 128 MiB of HBM per device.

v0:
```python
import jax
import jax.numpy as jnp
from jax import lax
from jax.sharding import Mesh
from jax.sharding import PartitionSpec as P

D = 2048
QK_DIM = 128
SSM_P = 64
STATE = 128
BLOCK = 128
KEY_BLOCK = 128
SP = ("sp_0", "sp_1")
FS_SP = ("fs", "sp_0", "sp_1")
FS_SP_TP = ("fs", "sp_0", "sp_1", "tp")


EPS = 1e-06
NEG = -1e30


def gathered_total(x, axis):
    return lax.all_gather(x, axis).sum(0)


def laid_out(parts, dim):
    lengths = list(parts.shape[1:])
    lengths[dim] *= parts.shape[0]
    return jnp.moveaxis(parts, 0, dim).reshape(lengths)


def copy_for_each(x, axis):
    length = lax.axis_size(axis)
    return lax.all_to_all(jnp.broadcast_to(x[None], (length, *x.shape)), axis, 0, 0, tiled=True)


def collect(x, axis, dim):
    return laid_out(copy_for_each(x, axis), dim)


def from_behind(x, axis, by):
    length = lax.axis_size(axis)
    pairs = [(i, i + by) for i in range(length) if 0 <= i + by < length]
    return lax.ppermute(x, axis, pairs)


def nothing_yet(x, identity):
    return jax.tree.map(
        lambda a, e: jnp.broadcast_to(jnp.asarray(e, a.dtype), a.shape), x, identity
    )


def prefix_by_axis(x, axes, combine, identity):
    before = start = nothing_yet(x, identity)
    running = x
    for axis in reversed(axes):
        length, index = (lax.axis_size(axis), lax.axis_index(axis))
        pieces = jax.tree.map(
            lambda part, kind: lax.all_gather(part.astype(kind), axis),
            running,
            (jnp.bfloat16, jnp.bfloat16),
        )
        inside, running = (start, start)
        for k in range(length):
            passed = k < index
            running = combine(
                running, jax.tree.map(lambda part, own: part[k].astype(own.dtype), pieces, x)
            )
            inside = jax.tree.map(lambda new, old: jnp.where(passed, new, old), running, inside)
        before = combine(inside, before)
    return before


def side_by_side(arrays, axis, dim, along):
    both = jnp.concatenate(arrays, axis=along)
    filled, at, gathered = (lax.all_gather(both, axis, axis=dim, tiled=True), 0, [])
    for a in arrays:
        gathered.append(lax.slice_in_dim(filled, at, at + a.shape[along], axis=along))
        at += a.shape[along]
    return tuple(gathered)


def per_device(
    hidden_in,
    in_gain,
    w_query,
    w_key,
    w_value,
    w_gate,
    w_inner,
    w_bvec,
    w_cvec,
    w_step,
    conv_inner,
    conv_bvec,
    conv_cvec,
    a_log,
    decay_add,
    lambdas,
    head_gain,
    ssm_gain,
    out_attn,
    out_ssm,
):
    rows_dev, half_width = hidden_in.shape
    in_float = hidden_in.astype(jnp.float32)
    squares = gathered_total(jnp.sum(in_float * in_float, axis=1), "tp")
    gain_half = lax.dynamic_slice_in_dim(in_gain, lax.axis_index("tp") * half_width, half_width, 0)
    normed = (in_float * lax.rsqrt(squares[:, None] / D + EPS) * gain_half[None, :]).astype(
        jnp.bfloat16
    )
    whole = collect(normed, "tp", 1)
    weight_list = (w_query, w_key, w_value, w_gate, w_inner, w_bvec, w_cvec, w_step)
    query, keys, values, gate_z, inner, b_pre, c_pre, step_pre = [
        jnp.dot(whole, weight, preferred_element_type=jnp.float32).astype(jnp.bfloat16)
        for weight in weight_list
    ]
    heads_att = lambdas.shape[0]
    first_row = lax.axis_index(SP) * rows_dev
    own_pos = first_row + jnp.arange(rows_dev, dtype=jnp.int32)
    scale = QK_DIM ** (-0.5)

    def head_major(rows_mat):
        return rows_mat.reshape(rows_mat.shape[0], heads_att * 2, QK_DIM).transpose(1, 0, 2)

    keys_major = head_major(keys)
    values_major = values.reshape(rows_dev, heads_att, 2 * QK_DIM).transpose(1, 0, 2)
    groups = [(head_major(query), own_pos)]
    start_states = tuple(
        (
            (
                jnp.full((heads_att, 2, group_pos.shape[0]), NEG, jnp.float32),
                jnp.zeros((heads_att, 2, group_pos.shape[0]), jnp.float32),
                jnp.zeros((heads_att, 2, group_pos.shape[0], 2 * QK_DIM), jnp.float32),
            )
            for group_query, group_pos in groups
        )
    )
    key_piece = lax.all_gather(keys_major, SP, axis=1, tiled=True)
    value_piece = lax.all_gather(values_major, SP, axis=1, tiled=True)

    def one_block(block_index, states):
        key_start = block_index * KEY_BLOCK
        key_rows = lax.dynamic_slice_in_dim(key_piece, block_index * KEY_BLOCK, KEY_BLOCK, 1)
        value_rows = lax.dynamic_slice_in_dim(value_piece, block_index * KEY_BLOCK, KEY_BLOCK, 1)
        key_pos = key_start + jnp.arange(KEY_BLOCK, dtype=jnp.int32)
        results = []
        for (group_query, group_pos), state in zip(groups, states):
            query_count = group_pos.shape[0]

            def update(current):
                peak, totals, accum = current
                scores = (
                    jnp.einsum(
                        "mqd,mkd->mqk", group_query, key_rows, preferred_element_type=jnp.float32
                    ).reshape(heads_att, 2, query_count, KEY_BLOCK)
                    * scale
                )
                visible = (key_pos[None, :] <= group_pos[:, None])[None, None]
                new_peak = jnp.maximum(peak, jnp.max(jnp.where(visible, scores, NEG), axis=-1))
                weights = jnp.where(visible, jnp.exp(scores - new_peak[..., None]), 0.0)
                shrink = jnp.exp(peak - new_peak)
                totals = totals * shrink + jnp.sum(weights, axis=-1)
                accum = accum * shrink[..., None] + jnp.einsum(
                    "hmqk,hke->hmqe",
                    weights.astype(jnp.bfloat16),
                    value_rows,
                    preferred_element_type=jnp.float32,
                )
                return (new_peak, totals, accum)

            results.append(
                lax.cond(key_start <= group_pos[-1], update, lambda unchanged: unchanged, state)
            )
        return tuple(results)

    finals = lax.fori_loop(0, key_piece.shape[1] // KEY_BLOCK, one_block, start_states)
    outputs = []
    for peak, totals, accum in finals:
        first_map = accum[:, 0] / totals[:, 0, :, None]
        second_map = accum[:, 1] / totals[:, 1, :, None]
        differ = first_map - lambdas[:, None, None] * second_map
        head_norm = (
            differ * lax.rsqrt(jnp.mean(differ * differ, axis=-1, keepdims=True) + EPS) * head_gain
        )
        outputs.append(
            head_norm.astype(jnp.bfloat16)
            .transpose(1, 0, 2)
            .reshape(accum.shape[2], heads_att * 2 * QK_DIM)
        )
    attn_out = outputs[0]
    heads_ssm = a_log.shape[0]
    groups_local = b_pre.shape[1] // STATE
    per_group = heads_ssm // groups_local
    stacked = jnp.concatenate([inner, b_pre, c_pre], axis=1)
    taps = conv_inner.shape[0]
    earlier = from_behind(stacked[rows_dev - (taps - 1) :], SP, 1)
    padded = jnp.concatenate([earlier, stacked], axis=0).astype(jnp.float32)
    conv_weight = jnp.concatenate([conv_inner, conv_bvec, conv_cvec], axis=1).astype(jnp.float32)
    summed = padded[0:rows_dev] * conv_weight[0]
    for offset in range(1, taps):
        summed = summed + padded[offset : offset + rows_dev] * conv_weight[offset]
    activated = jax.nn.silu(summed).astype(jnp.bfloat16)
    width_inner = inner.shape[1]
    width_vec = b_pre.shape[1]
    block_count = rows_dev // BLOCK
    inputs_x = activated[:, :width_inner].reshape(block_count, BLOCK, heads_ssm, SSM_P)
    inputs_b = activated[:, width_inner : width_inner + width_vec].reshape(
        block_count, BLOCK, groups_local, STATE
    )
    inputs_c = activated[:, width_inner + width_vec :].reshape(
        block_count, BLOCK, groups_local, STATE
    )
    step_size = jax.nn.softplus(step_pre.astype(jnp.float32))
    log_decay = -jnp.exp(a_log)[None, :] * step_size + decay_add
    size_major = step_size.reshape(block_count, BLOCK, heads_ssm).transpose(0, 2, 1)
    running = jnp.cumsum(
        log_decay.reshape(block_count, BLOCK, heads_ssm).transpose(0, 2, 1), axis=2
    )
    causal = jnp.tril(jnp.ones((BLOCK, BLOCK), dtype=bool))
    decay = jnp.exp(
        jnp.where(causal[None, None], running[:, :, :, None] - running[:, :, None, :], NEG)
    )
    intersection = jnp.einsum(
        "ntgk,nsgk->ngts", inputs_c, inputs_b, preferred_element_type=jnp.float32
    )
    matrix = (
        jnp.repeat(intersection, per_group, axis=1) * decay * size_major[:, :, None, :]
    ).astype(jnp.bfloat16)
    inside = jnp.einsum("nhts,nshp->nthp", matrix, inputs_x, preferred_element_type=jnp.float32)
    to_end = (jnp.exp(running[:, :, -1:] - running) * size_major).transpose(0, 2, 1)
    weighted = (inputs_x.astype(jnp.float32) * to_end[..., None]).astype(jnp.bfloat16)
    heads_b = jnp.repeat(inputs_b, per_group, axis=2)
    fresh = jnp.einsum("nshp,nshk->nhpk", weighted, heads_b, preferred_element_type=jnp.float32)
    block_totals = running[:, :, -1]

    def chain(state, items):
        fresh_block, total_block = items
        return (state * jnp.exp(total_block)[:, None, None] + fresh_block, state)

    local_end, local_enter = lax.scan(
        chain, jnp.zeros((heads_ssm, SSM_P, STATE), jnp.float32), (fresh, block_totals)
    )
    device_total = jnp.sum(block_totals, axis=0)

    def link(before, after):
        return (before[0] * jnp.exp(after[1])[:, None, None] + after[0], before[1] + after[1])

    incoming, skipped = prefix_by_axis(
        (local_end, device_total),
        SP,
        link,
        (jnp.zeros_like(local_end), jnp.zeros_like(device_total)),
    )
    preceding = jnp.concatenate(
        [jnp.zeros((1, heads_ssm), jnp.float32), jnp.cumsum(block_totals, axis=0)[:-1]], axis=0
    )
    entering = local_enter + incoming[None] * jnp.exp(preceding)[:, :, None, None]
    heads_c = jnp.repeat(inputs_c, per_group, axis=2).astype(jnp.float32)
    carried = (
        jnp.einsum("nthk,nhpk->nthp", heads_c, entering, precision=lax.Precision.HIGHEST)
        * jnp.exp(running).transpose(0, 2, 1)[..., None]
    )
    ssm_y = (inside + carried).reshape(rows_dev, heads_ssm * SSM_P)
    gated = (ssm_y * jax.nn.silu(gate_z.astype(jnp.float32))).reshape(rows_dev, groups_local, -1)
    grouped = gated * lax.rsqrt(jnp.mean(gated * gated, axis=-1, keepdims=True) + EPS)
    ssm_out = (grouped.reshape(rows_dev, heads_ssm * SSM_P) * ssm_gain).astype(jnp.bfloat16)
    attn_rows, ssm_rows = (
        lax.all_to_all(attn_out, "tp", split_axis=0, concat_axis=1, tiled=True),
        lax.all_to_all(ssm_out, "tp", split_axis=0, concat_axis=1, tiled=True),
    )
    full_attn, full_ssm = side_by_side((out_attn, out_ssm), "tp", 0, 1)
    joined = jnp.dot(attn_rows, full_attn, preferred_element_type=jnp.float32) + jnp.dot(
        ssm_rows, full_ssm, preferred_element_type=jnp.float32
    )
    return joined.astype(jnp.bfloat16)


def solution(mesh):
    split = Mesh(
        mesh.devices.reshape(4, 4, mesh.shape["fs"], mesh.shape["tp"]), ("sp_0", "sp_1", "fs", "tp")
    )
    in_specs = (
        P(FS_SP, "tp"),
        P(),
        P(None, "tp"),
        P(None, "tp"),
        P(None, "tp"),
        P(None, "tp"),
        P(None, "tp"),
        P(None, "tp"),
        P(None, "tp"),
        P(None, "tp"),
        P(None, "tp"),
        P(None, "tp"),
        P(None, "tp"),
        P("tp"),
        P(FS_SP, "tp"),
        P("tp"),
        P(),
        P("tp"),
        P("tp", None),
        P("tp", None),
    )
    out_specs = P(FS_SP_TP, None)
    return jax.shard_map(
        per_device, mesh=split, in_specs=in_specs, out_specs=out_specs, check_vma=False
    )
```

profile of v0, /device:TPU:127, one launch (start us, length us, event | category | flops | bytes accessed | tf_op | source)
XLA Modules:
  0.0 632.4 jit_solution(1211561122861284005)
XLA Ops:
  18.1 5.5 all_to_all.43
  43.7 7.7 %all-reduce.1 = bf16[32]{0:T(256)(128)(2,1)S(1)} all-reduce(bf16[32]{0:T(256)(128)(2,1)S(1)} %dynamic-update-slice), channel_id=3, replica_groups=mesh['sp_0'=4,'sp_1'=4,'fs'=4,'tp'=2] {'sp_1'}, use_global_device_ids=true, to_apply=%add.1 | all-reduce | flops 32 | bytes 128
  77.0 7.2 %while.31 = (s32[]{:T(128)}, f32[8,64,128]{2,1,0:T(8,128)S(1)}, f32[4,8,64,128]{3,2,1,0:T(8,128)}, f32[4,8]{1,0:T(4,128)S(1)}, f32[4,8,64,128]{3,2,1,0:T(8,128)}, /*index=5*/s32[]{:T(128)}, s32[]{:T(128)}) while((s32[]{:T(128)}, f32[8,64,128]{2,1,0:T(8,128)S(1)}, f32[4,8,64,128]{3,2,1,0:T(8,128)}, f32[4,8]{1,0:T(4,128)S(1)}, ...), condition=%wide.region_11.12_spmd.clone, body=%wide.region_10.11_spmd.clone.sunk | while | flops 262147 | bytes 1311424 | solution.py:241
  85.5 14.2 %all-gather.2 = bf16[32,64,128]{2,1,0:T(8,128)(2,1)S(1)} all-gather(bf16[8,64,128]{2,1,0:T(8,128)(2,1)S(1)} %convert_element_type.242), channel_id=4, replica_groups=mesh['sp_0'=4,'sp_1'=4,'fs'=4,'tp'=2] {'sp_1'}, dimensions={0}, use_global_device_ids=true | all-gather | bytes 655360 | tf_op jit(solution)/shard_map/all_gather | solution.py:59
  100.6 12.0 %all_gather.42 = bf16[4,8,64,128]{3,2,1,0:T(8,128)(2,1)S(1)} all-gather(bf16[1,8,64,128]{3,2,1,0:T(8,128)(2,1)S(1)} %fusion.62), channel_id=1, replica_groups=mesh['sp_0'=4,'sp_1'=4,'fs'=4,'tp'=2] {'sp_0'}, dimensions={0}, use_global_device_ids=true | all-gather | bytes 655360 | tf_op jit(solution)/shard_map/all_gather | solution.py:59
  134.0 10.5 %all_to_all.44 = bf16[2,256,512]{1,2,0:T(8,128)(2,1)S(1)} all-to-all(bf16[2,256,512]{1,2,0:T(8,128)(2,1)S(1)} %copy.107), channel_id=1, replica_groups=mesh['sp_0'=4,'sp_1'=4,'fs'=4,'tp'=2] {'tp'}, dimensions={0} | all-to-all | bytes 1048576 | tf_op jit(solution)/shard_map/all_to_all | solution.py:270
  149.3 34.8 %all-gather.9.cloned.1.call-done = bf16[4,8192,128]{2,1,0:T(8,128)(2,1)} async-done(((bf16[4,512,128]{2,1,0:T(8,128)(2,1)}), bf16[4,8192,128]{2,1,0:T(8,128)(2,1)}) %all-gather.9.cloned.1.call-update) | async-done | bytes 8388624 | tf_op jit(solution)/shard_map/all_gather | solution.py:139
  185.7 426.3 %while.30 = (s32[]{:T(128)}, f32[2,2,512]{2,1,0:T(2,128)S(1)}, f32[2,2,512]{2,1,0:T(2,128)S(1)}, f32[2,2,512,256]{3,2,1,0:T(8,128)}, s32[512]{0:T(512)S(1)}, /*i...) while((s32[]{:T(128)}, f32[2,2,512]{2,1,0:T(2,128)S(1)}, ...), condition=%wide.region_7.8_spmd, body=%wide.region_2.7_spmd.sunk | while | flops 204804224 | bytes 10801461 | solution.py:177
  193.8 5.3 conditional.2
  200.4 5.3 conditional.2
  207.1 5.3 conditional.2
  213.8 5.3 conditional.2
  220.4 5.3 conditional.2
  227.1 5.3 conditional.2
  233.7 5.3 conditional.2
  253.7 5.3 conditional.2
  273.7 5.3 conditional.2
  287.0 5.3 conditional.2
  307.0 5.3 conditional.2
  327.0 5.3 conditional.2
  360.3 5.3 conditional.2
  380.3 5.3 conditional.2
  400.3 5.3 conditional.2
  413.6 5.3 conditional.2
  433.6 5.3 conditional.2
  453.6 5.3 conditional.2
  486.9 5.3 conditional.2
  506.8 5.3 conditional.2
  526.8 5.3 conditional.2
  540.1 5.3 conditional.2
  560.1 5.3 conditional.2
  580.1 5.3 conditional.2
  (1166 shorter events, 695.8 us)
Async XLA Ops:
  6.5 118.4 %copy-start = (bf16[2048,512]{1,0:T(8,128)(2,1)S(1)}, bf16[2048,512]{1,0:T(8,128)(2,1)}, u32[]{:S(2)}) copy-start(bf16[2048,512]{1,0:T(8,128)(2,1)} %param.31) | copy-start | bytes 6291460
  6.5 138.0 %all-gather.13.cloned.1.call-start = ((), (), s32[]{:S(2)}) async-start(), calls=%async_computation.5 | async-start | bytes 12582912 | tf_op jit(solution)/shard_map/all_gather | solution.py:76
  11.4 1.2 copy-start.4
  11.4 137.9 %all-gather.11.cloned.1.call-start = ((), (), s32[]{:S(2)}) async-start(), calls=%async_computation.4 | async-start | bytes 8912896 | tf_op jit(solution)/shard_map/all_gather | solution.py:140
  18.0 6.9 %copy-start.25 = (bf16[2048,512]{1,0:T(8,128)(2,1)S(1)}, bf16[2048,512]{1,0:T(8,128)(2,1)}, u32[]{:S(2)}) copy-start(bf16[2048,512]{1,0:T(8,128)(2,1)} %param.30) | copy-start | bytes 6291460
  23.6 1.3 copy-start.2
  27.3 156.8 %all-gather.9.cloned.1.call-start = ((), (), s32[]{:S(2)}) async-start(), calls=%async_computation.3 | async-start | bytes 8912896 | tf_op jit(solution)/shard_map/all_gather | solution.py:139
  32.3 2.8 copy-start.3
  32.4 2.8 copy-start.27
  35.2 3.0 copy-start.8
  35.2 1.7 copy-start.26
  36.9 1.3 copy-start.9
  36.9 3.5 copy-start.28
  36.9 3.5 copy-start.14
  38.2 2.6 copy-start.15
  38.2 3.8 copy-start.29
  38.2 19.7 %copy-start.18 = (bf16[4,512]{1,0:T(4,128)(2,1)S(1)}, bf16[4,512]{1,0:T(4,128)(2,1)}, u32[]{:S(2)}) copy-start(bf16[4,512]{1,0:T(4,128)(2,1)} %param.36) | copy-start | bytes 12292
  38.2 19.7 %copy-start.19 = (bf16[4,256]{1,0:T(4,128)(2,1)S(1)}, bf16[4,256]{1,0:T(4,128)(2,1)}, u32[]{:S(2)}) copy-start(bf16[4,256]{1,0:T(4,128)(2,1)} %param.38) | copy-start | bytes 6148
  38.2 19.7 %copy-start.20 = (bf16[4,256]{1,0:T(4,128)(2,1)S(1)}, bf16[4,256]{1,0:T(4,128)(2,1)}, u32[]{:S(2)}) copy-start(bf16[4,256]{1,0:T(4,128)(2,1)} %param.37) | copy-start | bytes 6148
  39.1 27.0 %collective-permute-start = (bf16[3,1024]{0,1:T(8,128)(2,1)}, bf16[3,1024]{0,1:T(8,128)(2,1)}, u32[]{:S(2)}, u32[]{:S(2)}) collective-permute-start(bf16[3,1024]{0,1:T(8,128)(2,1)} %pad_maximum_fusion.1), channel_id=1, source_target_pairs={{0,8},{8,16},{16,24},{24,32},{32,40},{40,48},{48,56},{56,64},{64,7... | collective-permute-start | bytes 18440 | tf_op jit(solution)/shard_map/ppermute | solution.py:44
  40.8 23.4 %copy-start.10 = (f32[512,8]{0,1:T(8,128)}, f32[512,8]{0,1:T(8,128)S(1)}, u32[]{:S(2)}) copy-start(f32[512,8]{0,1:T(8,128)S(1)} %compare_select_fusion) | copy-start | bytes 49156
  113.7 1.0 copy-start.5
  113.7 1.0 copy-start.11
  114.7 1.2 copy-start.7
  114.7 1.2 copy-start.13
  114.7 1.2 copy-start.17
  132.3 1.3 copy-start.6
  132.3 1.2 copy-start.22
  149.3 36.4 %copy-start.12 = (s32[512]{0:T(512)S(1)}, s32[512]{0:T(512)}, u32[]{:S(2)}) copy-start(s32[512]{0:T(512)} %iota_add_fusion) | copy-start | bytes 6148
  185.7 426.4 %copy-start.24 = (f32[2]{0:T(128)S(1)}, f32[2]{0:T(128)}, u32[]{:S(2)}) copy-start(f32[2]{0:T(128)} %param.41) | copy-start | bytes 28
  612.1 2.1 copy-start.23
  620.6 5.3 copy-start.1
  (2 other events, 1.7 us)
Sparse Core Ops, SparseCore 0:
  11.5 24.0 all-gather.12
  37.8 73.6 all-gather.10
  113.6 70.4 all-gather.8
where the time goes:
time: 637 us; the launch traced here: 632 us
  matrix products  313 us (49%)
  local copies, waits for them, and re-layouts  106 us (17%)
  blocking collectives  62.5 us (10%)
  other arithmetic  50.5 us (8%)
  loops' own time  49.6 us (8%)
  waiting for transfers between devices  34.9 us (5%)
  between operations  14.3 us (2%)
    dot_general x64, matrix products, update(): jnp.einsum('hmqk,hke->hmqe', weights.astype(jnp.bfloat16), value_rows, pr...  196 us
    dot_general x64, matrix products, update(): jnp.einsum('mqd,mkd->mqk', group_query, key_rows, preferred_element_type=...  80.3 us
    another operation x1, loops' own time, per_device(): lax.fori_loop(0, key_piece.shape[1] // KEY_BLOCK, one_block, start_states)  44.8 us
    slice x64, local copies, waits for them, and re-layouts, one_block(): group_pos[-1]  42.2 us
    all_gather x1, waiting for transfers between devices, per_device(): key_piece = lax.all_gather(keys_major, SP, axis=1, tiled=True)  34.8 us
    all_gather x3, blocking collectives, prefix_by_axis(): lax.all_gather(part.astype(kind), axis)  31.5 us
    mul x64, local copies, waits for them, and re-layouts, update(): jnp.einsum('mqd,mkd->mqk', group_query, key_rows, preferred_element_type=...  20.7 us
    dot_general x8, matrix products, per_device(): jnp.dot(whole, weight, preferred_element_type=jnp.float32)  19.7 us
  transfers between devices with their start and end apart: 4, of which 1 were waited for; matrix products, arithmetic and copies ran while one was open for 12% of the time, Pallas kernels for 0%

commit v1 on v0

--- a/solution.py
+++ b/solution.py
@@ -1,6 +1,8 @@
 import jax
 import jax.numpy as jnp
 from jax import lax
+from jax.experimental import pallas as pl
+from jax.experimental.pallas import tpu as pltpu
 from jax.sharding import Mesh
 from jax.sharding import PartitionSpec as P
 
@@ -17,6 +19,263 @@
 
 EPS = 1e-06
 NEG = -1e30
+
+
+HALF = 256
+PAIR = 256
+MESH = pl.DeviceIdType.MESH
+ORDER = (0, 1, 3, 2)
+SCALE2 = QK_DIM ** (-0.5) * 1.4426950408889634
+
+
+def attention_kernel(
+    kv_in,
+    q_in,
+    lam_ref,
+    gain_ref,
+    out_ref,
+    kv,
+    q,
+    acc,
+    peak,
+    total,
+    done_out,
+    back,
+    zs_send,
+    zs_recv,
+    zq_send,
+    zq_recv,
+    ring_send,
+    kv_recv,
+    core_send,
+    back_send,
+    back_recv,
+):
+    z, y, c = lax.axis_index("sp_0"), lax.axis_index("sp_1"), lax.axis_index("tp")
+    right, left = lax.rem(y + 1, 4), lax.rem(y + 3, 4)
+    other = 1 - c
+    barrier = pltpu.get_barrier_semaphore()
+    for dz in range(4):
+        zz = lax.rem(z + dz, 4)
+        for dc in range(2):
+            if dz or dc:
+                pl.semaphore_signal(
+                    barrier,
+                    inc=1,
+                    device_id={"sp_0": zz, "tp": lax.rem(c + dc, 2)},
+                    device_id_type=MESH,
+                )
+    for yy in (left, right):
+        pl.semaphore_signal(barrier, inc=1, device_id={"sp_1": yy}, device_id_type=MESH)
+    pl.semaphore_wait(barrier, 9)
+
+    def exchange(src, dst_of, send, recv, j):
+        i, r = j // 2, j % 2
+        to = 2 * c + i
+        mine = jnp.logical_and(to == z, c == r)
+
+        @pl.when(mine)
+        def _():
+            pltpu.make_async_copy(src.at[j], dst_of(z), recv.at[z]).start()
+
+        @pl.when(jnp.logical_not(mine))
+        def _():
+            pltpu.make_async_remote_copy(
+                src_ref=src.at[j],
+                dst_ref=dst_of(z),
+                send_sem=send.at[j],
+                recv_sem=recv.at[z],
+                device_id={"sp_0": to, "tp": r},
+                device_id_type=MESH,
+            ).start()
+
+    for j in range(4):
+        exchange(kv_in, lambda zz: kv.at[0, zz], zs_send, zs_recv, j)
+    for j in range(4):
+        exchange(q_in, lambda zz: q.at[zz], zq_send, zq_recv, j)
+
+    acc[...] = jnp.zeros_like(acc)
+    total[...] = jnp.zeros_like(total)
+    peak[...] = jnp.full_like(peak, NEG)
+
+    def arrived(ref, sem):
+        pltpu.make_async_copy(ref, ref, sem).wait()
+
+    def to_neighbour(slot, zz, new_slot, yy, k):
+        return pltpu.make_async_remote_copy(
+            src_ref=kv.at[slot, zz],
+            dst_ref=kv.at[new_slot, zz],
+            send_sem=ring_send.at[k],
+            recv_sem=kv_recv.at[new_slot, zz],
+            device_id={"sp_1": yy},
+            device_id_type=MESH,
+        )
+
+    def to_partner(slot, zz):
+        return pltpu.make_async_remote_copy(
+            src_ref=kv.at[slot, zz],
+            dst_ref=kv.at[slot + 1, zz],
+            send_sem=core_send.at[slot // 2, zz],
+            recv_sem=kv_recv.at[slot + 1, zz],
+            device_id={"tp": other},
+            device_id_type=MESH,
+        )
+
+    def wait_chunk(slot, zz):
+        arrived(kv.at[slot, zz], kv_recv.at[slot, zz])
+
+    own = 2 * y + c
+
+    def block(zq, slot, zc, masked):
+        for m in range(2):
+            lanes = slice(m * QK_DIM, (m + 1) * QK_DIM)
+            scores = (
+                jnp.dot(
+                    kv[slot, zc, 0, :, lanes], q[zq, lanes, :], preferred_element_type=jnp.float32
+                )
+                * SCALE2
+            )
+            if masked:
+                key_at = lax.broadcasted_iota(jnp.int32, scores.shape, 0)
+                query_at = lax.broadcasted_iota(jnp.int32, scores.shape, 1)
+                scores = jnp.where(key_at <= query_at, scores, NEG)
+            old = peak[zq, m]
+            new = jnp.maximum(old, jnp.max(scores, axis=0, keepdims=True))
+            weights = jnp.exp2(scores - new[0:1])
+            shrink = jnp.exp2(old - new)
+            peak[zq, m] = new
+            total[zq, m] = total[zq, m] * shrink + jnp.sum(weights, axis=0, keepdims=True)
+            acc[zq, m] = acc[zq, m] * shrink[0:1] + jnp.dot(
+                kv[slot, zc, 1], weights.astype(jnp.bfloat16), preferred_element_type=jnp.float32
+            )
+
+    def chunk(slot, zc):
+        if slot == 0:
+            block(zc, slot, zc, True)
+            low = zc + 1
+        else:
+            theirs = 2 * lax.rem(y + slot // 2, 4) + (c if slot % 2 == 0 else other)
+            low = zc + jnp.where(theirs > own, 1, 0)
+
+        def step(zq, carry):
+            block(zq, slot, zc, False)
+            return carry
+
+        lax.fori_loop(low, 4, step, 0)
+
+    at = [lax.rem(z + d, 4) for d in ORDER]
+    for t in range(4):
+        arrived(kv.at[0, at[t]], zs_recv.at[at[t]])
+        to_neighbour(0, at[t], 6, right, t).start()
+        to_neighbour(0, at[t], 2, left, 4 + t).start()
+        to_partner(0, at[t]).start()
+    for t in range(4):
+        arrived(q.at[at[t]], zq_recv.at[at[t]])
+
+    def over(slot, t):
+        chunk(slot, at[t])
+
+    for t in range(4):
+        over(0, t)
+    for t in range(4):
+        wait_chunk(1, at[t])
+        over(1, t)
+    for t in range(4):
+        wait_chunk(6, at[t])
+        if t < 2:
+            to_neighbour(6, at[t], 4, right, 8 + t).start()
+        to_partner(6, at[t]).start()
+        wait_chunk(2, at[t])
+        if t >= 2:
+            to_neighbour(2, at[t], 4, left, 8 + t).start()
+        to_partner(2, at[t]).start()
+        over(6, t)
+        over(2, t)
+        if t:
+            wait_chunk(7, at[t - 1])
+            over(7, t - 1)
+            wait_chunk(3, at[t - 1])
+            over(3, t - 1)
+    wait_chunk(7, at[3])
+    over(7, 3)
+    wait_chunk(3, at[3])
+    over(3, 3)
+    for t in (0, 2, 1, 3):
+        wait_chunk(4, at[t])
+        to_partner(4, at[t]).start()
+        over(4, t)
+    for t in (0, 2, 1, 3):
+        wait_chunk(5, at[t])
+        over(5, t)
+
+    for dz in ORDER:
+        zz = lax.rem(z + dz, 4)
+        differ = acc[zz, 0] / total[zz, 0, 0:1] - lam_ref[0:1] * (acc[zz, 1] / total[zz, 1, 0:1])
+        scale = lax.rsqrt(jnp.mean(differ * differ, axis=0, keepdims=True) + EPS)
+        done_out[zz] = (differ * scale * gain_ref[...]).astype(jnp.bfloat16)
+        if dz == 0:
+            pltpu.make_async_copy(done_out.at[zz], back.at[z], back_recv.at[z]).start()
+        else:
+            pltpu.make_async_remote_copy(
+                src_ref=done_out.at[zz],
+                dst_ref=back.at[z],
+                send_sem=back_send.at[dz],
+                recv_sem=back_recv.at[z],
+                device_id={"sp_0": zz},
+                device_id_type=MESH,
+            ).start()
+    for dz in (0, 1, 3, 2):
+        zz = lax.rem(z + dz, 4)
+        arrived(back.at[zz], back_recv.at[zz])
+        out_ref[zz] = back[zz]
+
+    for j in range(4):
+        mine = jnp.logical_and(2 * c + j // 2 == z, c == j % 2)
+
+        @pl.when(jnp.logical_not(mine))
+        def _():
+            arrived(kv_in.at[j], zs_send.at[j])
+            arrived(q_in.at[j], zq_send.at[j])
+
+    for k in range(12):
+        arrived(kv.at[0, 0], ring_send.at[k])
+    for s in range(4):
+        for t in range(4):
+            arrived(kv.at[0, 0], core_send.at[s, t])
+    for dz in range(1, 4):
+        arrived(done_out.at[0], back_send.at[dz])
+
+
+def attention(kv_in, q_in, lam_tile, gain_col):
+    vmem = pl.BlockSpec(memory_space=pltpu.VMEM)
+    dma = pltpu.SemaphoreType.DMA
+    return pl.pallas_call(
+        attention_kernel,
+        out_shape=jax.ShapeDtypeStruct((4, PAIR, HALF), jnp.bfloat16),
+        in_specs=[vmem] * 4,
+        out_specs=vmem,
+        scratch_shapes=[
+            pltpu.VMEM((8, 4, 2, HALF, PAIR), jnp.bfloat16),
+            pltpu.VMEM((4, PAIR, HALF), jnp.bfloat16),
+            pltpu.VMEM((4, 2, PAIR, HALF), jnp.float32),
+            pltpu.VMEM((4, 2, 8, HALF), jnp.float32),
+            pltpu.VMEM((4, 2, 8, HALF), jnp.float32),
+            pltpu.VMEM((4, PAIR, HALF), jnp.bfloat16),
+            pltpu.VMEM((4, PAIR, HALF), jnp.bfloat16),
+            dma((4,)),
+            dma((4,)),
+            dma((4,)),
+            dma((4,)),
+            dma((12,)),
+            dma((8, 4)),
+            dma((4, 4)),
+            dma((4,)),
+            dma((4,)),
+        ],
+        compiler_params=pltpu.CompilerParams(
+            collective_id=0, has_side_effects=True, vmem_limit_bytes=40 * 2**20
+        ),
+    )(kv_in, q_in, lam_tile, gain_col)
 
 
 def gathered_total(x, axis):
@@ -115,80 +374,30 @@
         jnp.dot(whole, weight, preferred_element_type=jnp.float32).astype(jnp.bfloat16)
         for weight in weight_list
     ]
-    heads_att = lambdas.shape[0]
-    first_row = lax.axis_index(SP) * rows_dev
-    own_pos = first_row + jnp.arange(rows_dev, dtype=jnp.int32)
-    scale = QK_DIM ** (-0.5)
-
-    def head_major(rows_mat):
-        return rows_mat.reshape(rows_mat.shape[0], heads_att * 2, QK_DIM).transpose(1, 0, 2)
-
-    keys_major = head_major(keys)
-    values_major = values.reshape(rows_dev, heads_att, 2 * QK_DIM).transpose(1, 0, 2)
-    groups = [(head_major(query), own_pos)]
-    start_states = tuple(
-        (
-            (
-                jnp.full((heads_att, 2, group_pos.shape[0]), NEG, jnp.float32),
-                jnp.zeros((heads_att, 2, group_pos.shape[0]), jnp.float32),
-                jnp.zeros((heads_att, 2, group_pos.shape[0], 2 * QK_DIM), jnp.float32),
+    kv_in = jnp.stack(
+        [
+            jnp.stack(
+                [
+                    keys[r * HALF : (r + 1) * HALF, i * PAIR : (i + 1) * PAIR],
+                    values[r * HALF : (r + 1) * HALF, i * PAIR : (i + 1) * PAIR].T,
+                ]
             )
-            for group_query, group_pos in groups
-        )
-    )
-    key_piece = lax.all_gather(keys_major, SP, axis=1, tiled=True)
-    value_piece = lax.all_gather(values_major, SP, axis=1, tiled=True)
-
-    def one_block(block_index, states):
-        key_start = block_index * KEY_BLOCK
-        key_rows = lax.dynamic_slice_in_dim(key_piece, block_index * KEY_BLOCK, KEY_BLOCK, 1)
-        value_rows = lax.dynamic_slice_in_dim(value_piece, block_index * KEY_BLOCK, KEY_BLOCK, 1)
-        key_pos = key_start + jnp.arange(KEY_BLOCK, dtype=jnp.int32)
-        results = []
-        for (group_query, group_pos), state in zip(groups, states):
-            query_count = group_pos.shape[0]
-
-            def update(current):
-                peak, totals, accum = current
-                scores = (
-                    jnp.einsum(
-                        "mqd,mkd->mqk", group_query, key_rows, preferred_element_type=jnp.float32
-                    ).reshape(heads_att, 2, query_count, KEY_BLOCK)
-                    * scale
-                )
-                visible = (key_pos[None, :] <= group_pos[:, None])[None, None]
-                new_peak = jnp.maximum(peak, jnp.max(jnp.where(visible, scores, NEG), axis=-1))
-                weights = jnp.where(visible, jnp.exp(scores - new_peak[..., None]), 0.0)
-                shrink = jnp.exp(peak - new_peak)
-                totals = totals * shrink + jnp.sum(weights, axis=-1)
-                accum = accum * shrink[..., None] + jnp.einsum(
-                    "hmqk,hke->hmqe",
-                    weights.astype(jnp.bfloat16),
-                    value_rows,
-                    preferred_element_type=jnp.float32,
-                )
-                return (new_peak, totals, accum)
-
-            results.append(
-                lax.cond(key_start <= group_pos[-1], update, lambda unchanged: unchanged, state)
-            )
-        return tuple(results)
-
-    finals = lax.fori_loop(0, key_piece.shape[1] // KEY_BLOCK, one_block, start_states)
-    outputs = []
-    for peak, totals, accum in finals:
-        first_map = accum[:, 0] / totals[:, 0, :, None]
-        second_map = accum[:, 1] / totals[:, 1, :, None]
-        differ = first_map - lambdas[:, None, None] * second_map
-        head_norm = (
-            differ * lax.rsqrt(jnp.mean(differ * differ, axis=-1, keepdims=True) + EPS) * head_gain
-        )
-        outputs.append(
-            head_norm.astype(jnp.bfloat16)
-            .transpose(1, 0, 2)
-            .reshape(accum.shape[2], heads_att * 2 * QK_DIM)
-        )
-    attn_out = outputs[0]
+            for i in range(2)
+            for r in range(2)
+        ]
+    )
+    q_in = jnp.stack(
+        [
+            query[r * HALF : (r + 1) * HALF, i * PAIR : (i + 1) * PAIR].T
+            for i in range(2)
+            for r in range(2)
+        ]
+    )
+    lam_all = lax.all_gather(lambdas, "tp", tiled=True)
+    lam_tile = jnp.broadcast_to(
+        lax.dynamic_slice_in_dim(lam_all, lax.axis_index("sp_0"), 1, 0)[:, None], (8, 256)
+    )
+    attn_cols = attention(kv_in, q_in, lam_tile, head_gain.reshape(PAIR, 1))
     heads_ssm = a_log.shape[0]
     groups_local = b_pre.shape[1] // STATE
     per_group = heads_ssm // groups_local
@@ -265,14 +474,11 @@
     gated = (ssm_y * jax.nn.silu(gate_z.astype(jnp.float32))).reshape(rows_dev, groups_local, -1)
     grouped = gated * lax.rsqrt(jnp.mean(gated * gated, axis=-1, keepdims=True) + EPS)
     ssm_out = (grouped.reshape(rows_dev, heads_ssm * SSM_P) * ssm_gain).astype(jnp.bfloat16)
-    attn_rows, ssm_rows = (
-        lax.all_to_all(attn_out, "tp", split_axis=0, concat_axis=1, tiled=True),
-        lax.all_to_all(ssm_out, "tp", split_axis=0, concat_axis=1, tiled=True),
-    )
+    ssm_rows = lax.all_to_all(ssm_out, "tp", split_axis=0, concat_axis=1, tiled=True)
     full_attn, full_ssm = side_by_side((out_attn, out_ssm), "tp", 0, 1)
-    joined = jnp.dot(attn_rows, full_attn, preferred_element_type=jnp.float32) + jnp.dot(
-        ssm_rows, full_ssm, preferred_element_type=jnp.float32
-    )
+    joined = jnp.einsum(
+        "hcq,hcd->qd", attn_cols, full_attn.reshape(4, PAIR, D), preferred_element_type=jnp.float32
+    ) + jnp.dot(ssm_rows, full_ssm, preferred_element_type=jnp.float32)
     return joined.astype(jnp.bfloat16)
 
 

time: 637 us -> 254 us (0.40)
  the two profiles are of different devices: /device:TPU:127 before, /device:TPU:1 now
where the time goes in v1:
time: 254 us; the launch traced here: 249 us
  Pallas kernels  70.7 us (28%)
  blocking collectives  61.3 us (24%)
  local copies, waits for them, and re-layouts  37 us (15%)
  matrix products  27.9 us (11%)
  other arithmetic  24.5 us (10%)
  between operations  15.6 us (6%)
  starting transfers between devices  11.9 us (5%)
    pallas_call x1, Pallas kernels, attention(): pl.pallas_call(attention_kernel, out_shape=jax.ShapeDtypeStruct((4, PAIR,...  70.7 us
    all_gather x3, blocking collectives, prefix_by_axis(): lax.all_gather(part.astype(kind), axis)  37.1 us
    unnamed x2, blocking collectives  15.8 us
    dot_general x8, matrix products, per_device(): jnp.dot(whole, weight, preferred_element_type=jnp.float32)  15.4 us
    unnamed x125, local copies, waits for them, and re-layouts  10.7 us
    all_to_all x1, starting transfers between devices, per_device(): lax.all_to_all(ssm_out, 'tp', split_axis=0, concat_axis=1, tiled=True)  7.94 us
    all_to_all x1, blocking collectives, copy_for_each(): lax.all_to_all(jnp.broadcast_to(x[None], (length, *x.shape)), axis, 0, 0,...  5.52 us
    dot_general x1, matrix products, per_device(): jnp.dot(ssm_rows, full_ssm, preferred_element_type=jnp.float32)  5.11 us
  transfers between devices with their start and end apart: 3, of which 0 were waited for; matrix products, arithmetic and copies ran while one was open for 26% of the time, Pallas kernels for 28%

profile of v1, /device:TPU:1, one launch (start us, length us, event | category | flops | bytes accessed | tf_op | source)
XLA Modules:
  0.0 249.1 jit_solution(47682942812723677)
XLA Ops:
  6.5 1.7 fusion.10
  8.2 2.9 %all-gather.3 = f32[2,1,512]{2,1,0:T(1,128)S(1)} all-gather(f32[1,1,512]{2,1,0:T(1,128)S(1)} %bitcast.197), channel_id=2, replica_groups=mesh['sp_0'=4,'sp_1'=4,'fs'=4,'tp'=2] {'tp'}, dimensions={0}, use_global_device_ids=true | all-gather | bytes 6144 | tf_op jit(solution)/shard_map/all_gather | solution.py:282
  11.8 2.5 %fusion.12 = bf16[512,1024]{1,0:T(8,128)(2,1)} fusion(bf16[512,1024]{1,0:T(8,128)(2,1)} %param.22, f32[1024]{0:T(1024)S(1)} %dynamic_slice.14, f32[512]{0:T(512)S(1)} %add_rsqrt_fusion.1), kind=kLoop, calls=%fused_computation.15 | loop fusion | flops 2097152 | bytes 2103296 | tf_op jit(solution)/shard_map/convert_element_type | solution.py:368
  14.3 1.5 copy.73
  16.0 5.5 %all_to_all.24 = bf16[2,512,1024]{1,2,0:T(8,128)(2,1)S(1)} all-to-all(bf16[2,512,1024]{1,2,0:T(8,128)(2,1)S(1)} %broadcast_in_dim.31), channel_id=1, replica_groups=mesh['sp_0'=4,'sp_1'=4,'fs'=4,'tp'=2] {'tp'}, dimensions={0} | all-to-all | bytes 4194304 | tf_op jit(solution)/shard_map/all_to_all | solution.py:293
  28.1 4.0 %collective-permute-start = (bf16[3,1024]{0,1:T(8,128)(2,1)}, bf16[3,1024]{0,1:T(8,128)(2,1)}, u32[]{:S(2)}, u32[]{:S(2)}) collective-permute-start(bf16[3,1024]{0,1:T(8,128)(2,1)} %pad_maximum_fusion.3), channel_id=1, source_target_pairs={{0,8},{8,16},{16,24},{24,32},{32,40},{40,48},{48,56},{56,64},{64,7... | collective-permute-start | bytes 18440 | tf_op jit(solution)/shard_map/ppermute | solution.py:303
  32.1 2.6 %pad_maximum_fusion = bf16[512,4096]{1,0:T(8,128)(2,1)} fusion(bf16[512,2048]{1,0:T(8,128)(2,1)S(1)} %copy-done.13, bf16[512,2048]{1,0:T(8,128)(2,1)S(1)} %copy-done.14), kind=kLoop, calls=%fused_computation.7 | loop fusion | flops 8388608 | bytes 8388608 | tf_op jit(solution)/shard_map/concatenate | solution.py:334
  36.5 2.0 compare_select_fusion
  41.5 8.0 %all-reduce.2 = bf16[32]{0:T(256)(128)(2,1)S(1)} all-reduce(bf16[32]{0:T(256)(128)(2,1)S(1)} %dynamic-update-slice.1), channel_id=3, replica_groups=mesh['sp_0'=4,'sp_1'=4,'fs'=4,'tp'=2] {'sp_1'}, use_global_device_ids=true, to_apply=%add.2 | all-reduce | flops 32 | bytes 128
  50.1 7.5 %all-gather.4 = bf16[4,1,8]{2,1,0:T(2,128)(2,1)} all-gather(bf16[1,1,8]{2,1,0:T(2,128)(2,1)S(1)} %get-tuple-element.65), channel_id=1, replica_groups=mesh['sp_0'=4,'sp_1'=4,'fs'=4,'tp'=2] {'sp_0'}, dimensions={0}, use_global_device_ids=true | all-gather | bytes 80 | tf_op jit(solution)/shard_map/all_gather | solution.py:318
  58.2 3.7 %convolution_convert_fusion.2 = bf16[512,512]{0,1:T(8,128)(2,1)S(1)} fusion(bf16[512,2048]{0,1:T(8,128)(2,1)} %bitcast.180, bf16[2048,512]{1,0:T(8,128)(2,1)} %param.24), kind=kOutput, calls=%fused_computation.34 | convolution fusion | flops 1074003968 | bytes 4718592 | tf_op jit(solution)/shard_map/dot_general | solution.py:374
  62.6 1.3 convolution_convert_fusion.3
  66.6 1.3 dynamic-update-slice
  68.0 1.8 pad_maximum_fusion.2.q_in
  74.9 7.8 %all-reduce.1 = f32[4]{0:T(128)} all-reduce(f32[4]{0:T(128)S(1)} %copy-done.58), channel_id=1, replica_groups=mesh['sp_0'=4,'sp_1'=4,'fs'=4,'tp'=2] {'tp'}, use_global_device_ids=true, to_apply=%add.1 | all-reduce | flops 4 | bytes 32
  86.4 70.7 %shard_map.190 = bf16[4,256,256]{2,1,0:T(8,128)(2,1)S(1)} custom-call(bf16[4,2,256,256]{3,2,1,0:T(8,128)(2,1)S(1)} %pad_maximum_fusion.1.kv_in, bf16[4,256,256]{2,1,0:T(8,128)(2,1)S(1)} %copy-done.1, f32[8,256]{1,0:T(8,128)S(1)} %broadcast_in_dim.35.lam_ref, f32[256,1]{1,0:T(8,128)S(1)} %copy.76.gain_ref), custom_call_target="tpu_custom_call" | custom-call | tf_op jit(solution)/shard_map/pallas_call | solution.py:252
  157.1 1.6 maximum_convert_fusion
  158.8 2.6 %multiply_convert_fusion.1 = bf16[512,1024]{0,1:T(8,128)(2,1)S(1)} fusion(f32[515,1024]{0,1:T(8,128)S(1)} %maximum_convert_fusion, f32[1024]{0:T(1024)S(1)} %bitcast.194, f32[1024]{0:T(1024)S(1)} %bitcast.195, f32[1024]{0:T(1024)S(1)} %bitcast.196, f32[1024]{0:T(1024)S(1)} %bitcast.193), kind=kLoop, calls=%fused_computation.24 | loop fusion | flops 6291456 | bytes 9453568 | tf_op jit(solution)/shard_map/convert_element_type | solution.py:412
  162.2 2.0 reshape.193
  168.5 1.4 fusion.30
  170.0 5.9 %while.13 = (s32[]{:T(128)}, f32[8,64,128]{2,1,0:T(8,128)S(1)}, f32[4,8,64,128]{3,2,1,0:T(8,128)}, f32[4,8]{1,0:T(4,128)}, f32[4,8,64,128]{3,2,1,0:T(8,128)S(1)}, /*index=5*/s32[]{:T(128)}, s32[]{:T(128)}) while((s32[]{:T(128)}, f32[8,64,128]{2,1,0:T(8,128)S(1)}, f32[4,8,64,128]{3,2,1,0:T(8,128)}, f32[4,8]{1,0:T(4,128)}, ...), condition=%wide.region_4.5_spmd.clone, body=%wide.region_3.4_spmd.clone.sunk | while | flops 262147 | bytes 1310924 | solution.py:450
  176.0 19.7 %all-gather.2 = bf16[32,64,128]{2,1,0:T(8,128)(2,1)S(1)} all-gather(bf16[8,64,128]{2,1,0:T(8,128)(2,1)S(1)} %convert_element_type.225), channel_id=4, replica_groups=mesh['sp_0'=4,'sp_1'=4,'fs'=4,'tp'=2] {'sp_1'}, dimensions={0}, use_global_device_ids=true | all-gather | bytes 655360 | tf_op jit(solution)/shard_map/all_gather | solution.py:318
  195.9 9.9 %all_gather.38 = bf16[4,8,64,128]{3,2,1,0:T(8,128)(2,1)S(1)} all-gather(bf16[1,8,64,128]{3,2,1,0:T(8,128)(2,1)S(1)} %fusion.43), channel_id=1, replica_groups=mesh['sp_0'=4,'sp_1'=4,'fs'=4,'tp'=2] {'sp_0'}, dimensions={0}, use_global_device_ids=true | all-gather | bytes 655360 | tf_op jit(solution)/shard_map/all_gather | solution.py:318
  208.6 2.2 fusion.17
  210.8 1.9 copy.92
  212.7 1.9 reshape.284
  214.7 4.4 %fusion.57 = (f32[512,512]{1,0:T(8,128)}, f32[512,512]{1,0:T(8,128)}) fusion(f32[512,512]{1,0:T(8,128)S(1)} %reshape.284, bf16[512,2048]{0,1:T(8,128)(2,1)} %bitcast.181, bf16[2048,512]{1,0:T(8,128)(2,1)S(1)} %copy-done), kind=kOutput, calls=%fused_computation.137 | convolution fusion | flops 1075838976 | bytes 7340032 | tf_op jit(solution)/shard_map/dot_general | solution.py:374
  219.0 1.9 mul.288
  224.0 7.9 %all-to-all-start.1 = ((bf16[2,256,512]{1,2,0:T(8,128)(2,1)}), bf16[2,256,512]{1,2,0:T(8,128)(2,1)S(1)}, u32[]{:S(2)}, u32[]{:S(2)}) async-start(bf16[2,256,512]{1,2,0:T(8,128)(2,1)} %copy.88), calls=%async_computation.1 | async-start | bytes 1048576 | tf_op jit(solution)/shard_map/all_to_all | solution.py:477
  233.0 1.3 slice-done
  234.3 2.6 %convolution_bitcast_fusion = f32[256,2048]{1,0:T(8,128)} fusion(bf16[4,256,256]{2,1,0:T(8,128)(2,1)S(1)} %copy-done.3, bf16[4,256,2048]{2,1,0:T(8,128)(2,1)S(1)} %bitcast.184), kind=kOutput, calls=%fused_computation.8 | convolution fusion | flops 1073741824 | bytes 6815744 | tf_op jit(solution)/shard_map/hcq,hcd->qd/dot_general | solution.py:479
  236.9 5.1 %fusion.7 = bf16[256,2048]{1,0:T(8,128)(2,1)} fusion(f32[256,2048]{1,0:T(8,128)} %convolution_bitcast_fusion, bf16[256,1024]{0,1:T(8,128)(2,1)S(1)} %bitcast.191, bf16[1024,4096]{1,0:T(8,128)(2,1)} %all-gather.7.cloned.1.call-done), kind=kOutput, calls=%fused_computation.12 | convolution fusion | flops 1074790400 | bytes 7864320 | tf_op jit(solution)/shard_map/dot_general | solution.py:481
  (195 shorter events, 42.3 us)
Async XLA Ops:
  6.5 208.1 %copy-start = (bf16[2048,512]{1,0:T(8,128)(2,1)S(1)}, bf16[2048,512]{1,0:T(8,128)(2,1)}, u32[]{:S(2)}) copy-start(bf16[2048,512]{1,0:T(8,128)(2,1)} %param.27) | copy-start | bytes 6291460
  6.5 225.4 %all-gather.7.cloned.1.call-start = ((), (), s32[]{:S(2)}) async-start(), calls=%async_computation.2 | async-start | bytes 12582912 | tf_op jit(solution)/shard_map/all_gather | solution.py:335
  15.9 5.5 %copy-start.53 = (bf16[2048,256]{1,0:T(8,128)(2,1)S(1)}, bf16[2048,256]{1,0:T(8,128)(2,1)}, u32[]{:S(2)}) copy-start(bf16[2048,256]{1,0:T(8,128)(2,1)} %param.30) | copy-start | bytes 3145732
  25.1 7.0 %copy-start.13 = (bf16[512,2048]{1,0:T(8,128)(2,1)S(1)}, bf16[512,2048]{1,0:T(8,128)(2,1)}, u32[]{:S(2)}) copy-start(bf16[512,2048]{1,0:T(8,128)(2,1)} %param.41) | copy-start | bytes 6291460
  25.1 7.0 %copy-start.14 = (bf16[512,2048]{1,0:T(8,128)(2,1)S(1)}, bf16[512,2048]{1,0:T(8,128)(2,1)}, u32[]{:S(2)}) copy-start(bf16[512,2048]{1,0:T(8,128)(2,1)} %param.40) | copy-start | bytes 6291460
  28.1 129.0 %collective-permute-start = (bf16[3,1024]{0,1:T(8,128)(2,1)}, bf16[3,1024]{0,1:T(8,128)(2,1)}, u32[]{:S(2)}, u32[]{:S(2)}) collective-permute-start(bf16[3,1024]{0,1:T(8,128)(2,1)} %pad_maximum_fusion.3), channel_id=1, source_target_pairs={{0,8},{8,16},{16,24},{24,32},{32,40},{40,48},{48,56},{56,64},{64,7... | collective-permute-start | bytes 18440 | tf_op jit(solution)/shard_map/ppermute | solution.py:303
  34.7 4.4 %copy-start.35 = (f32[512,8]{0,1:T(8,128)S(1)}, f32[512,8]{0,1:T(8,128)}, u32[]{:S(2)}) copy-start(f32[512,8]{0,1:T(8,128)} %param.36) | copy-start | bytes 49156
  40.5 21.4 %copy-start.29 = (f32[4,8]{1,0:T(4,128)}, f32[4,8]{1,0:T(4,128)S(1)}, u32[]{:S(2)}) copy-start(f32[4,8]{1,0:T(4,128)S(1)} %get-tuple-element.134) | copy-start | bytes 388
  49.5 12.4 %copy-start.27 = (bf16[32]{0:T(256)(128)(2,1)}, bf16[32]{0:T(256)(128)(2,1)S(1)}, u32[]{:S(2)}) copy-start(bf16[32]{0:T(256)(128)(2,1)S(1)} %all-reduce.2) | copy-start | bytes 196
  58.2 4.4 %copy-start.5 = (bf16[2,512,1024]{1,2,0:T(8,128)(2,1)S(1)}, bf16[2,512,1024]{1,2,0:T(8,128)(2,1)}, u32[]{:S(2)}) copy-start(bf16[2,512,1024]{1,2,0:T(8,128)(2,1)} %copy-done.4) | copy-start | bytes 6291460
  58.2 4.4 %copy-start.52 = (bf16[2048,512]{1,0:T(8,128)(2,1)S(1)}, bf16[2048,512]{1,0:T(8,128)(2,1)}, u32[]{:S(2)}) copy-start(bf16[2048,512]{1,0:T(8,128)(2,1)} %param.26) | copy-start | bytes 6291460
  70.5 3.0 %copy-start.22 = (f32[512,8]{0,1:T(8,128)S(1)}, f32[512,8]{0,1:T(8,128)}, u32[]{:S(2)}) copy-start(f32[512,8]{0,1:T(8,128)} %copy-done.21) | copy-start | bytes 49156
  70.5 3.0 %copy-start.30 = (f32[4,8]{1,0:T(4,128)S(1)}, f32[4,8]{1,0:T(4,128)}, u32[]{:S(2)}) copy-start(f32[4,8]{1,0:T(4,128)} %copy-done.29) | copy-start | bytes 388
  70.5 3.7 %copy-start.39 = (f32[4,8]{1,0:T(4,128)S(1)}, f32[4,8]{1,0:T(4,128)}, u32[]{:S(2)}) copy-start(f32[4,8]{1,0:T(4,128)} %reduce_window_sum.23) | copy-start | bytes 388
  70.6 4.3 %copy-start.58 = (f32[4]{0:T(128)S(1)}, f32[4]{0:T(128)}, u32[]{:S(2)}) copy-start(f32[4]{0:T(128)} %dynamic-update-slice) | copy-start | bytes 52
  86.4 70.7 %copy-start.10 = (bf16[512,512]{0,1:T(8,128)(2,1)S(1)}, bf16[512,512]{0,1:T(8,128)(2,1)}, u32[]{:S(2)}) copy-start(bf16[512,512]{0,1:T(8,128)(2,1)} %copy-done.9) | copy-start | bytes 1572868
  86.4 70.8 %copy-start.18 = (bf16[512,256]{0,1:T(8,128)(2,1)S(1)}, bf16[512,256]{0,1:T(8,128)(2,1)}, u32[]{:S(2)}) copy-start(bf16[512,256]{0,1:T(8,128)(2,1)} %copy-done.17) | copy-start | bytes 786436
  86.4 70.8 %copy-start.20 = (bf16[512,256]{0,1:T(8,128)(2,1)S(1)}, bf16[512,256]{0,1:T(8,128)(2,1)}, u32[]{:S(2)}) copy-start(bf16[512,256]{0,1:T(8,128)(2,1)} %copy-done.19) | copy-start | bytes 786436
  157.0 4.4 %copy-start.2 = (bf16[4,256,256]{2,1,0:T(8,128)(2,1)}, bf16[4,256,256]{2,1,0:T(8,128)(2,1)S(1)}, u32[]{:S(2)}) copy-start(bf16[4,256,256]{2,1,0:T(8,128)(2,1)S(1)} %shard_map.190) | copy-start | bytes 1572868
  164.2 4.3 %copy-start.24 = (f32[4,128,8]{1,2,0:T(8,128)S(1)}, f32[4,128,8]{1,2,0:T(8,128)}, u32[]{:S(2)}) copy-start(f32[4,128,8]{1,2,0:T(8,128)} %bitcast_multiply_fusion) | copy-start | bytes 49156
  170.0 25.7 %copy-start.40 = (f32[8]{0:T(128)S(1)}, f32[8]{0:T(128)}, u32[]{:S(2)}) copy-start(f32[8]{0:T(128)} %get-tuple-element.90) | copy-start | bytes 100
  170.0 25.7 %copy-start.41 = (f32[8]{0:T(128)S(1)}, f32[8]{0:T(128)}, u32[]{:S(2)}) copy-start(f32[8]{0:T(128)} %get-tuple-element.91) | copy-start | bytes 100
  170.0 25.7 %copy-start.42 = (f32[8]{0:T(128)S(1)}, f32[8]{0:T(128)}, u32[]{:S(2)}) copy-start(f32[8]{0:T(128)} %get-tuple-element.92) | copy-start | bytes 100
  170.0 25.7 %copy-start.43 = (f32[8]{0:T(128)S(1)}, f32[8]{0:T(128)}, u32[]{:S(2)}) copy-start(f32[8]{0:T(128)} %get-tuple-element.93) | copy-start | bytes 100
  175.9 29.9 %copy-start.44 = (f32[8]{0:T(128)S(1)}, f32[8]{0:T(128)}, u32[]{:S(2)}) copy-start(f32[8]{0:T(128)} %get-tuple-element.89) | copy-start | bytes 100
  175.9 29.9 %copy-start.45 = (f32[8]{0:T(128)S(1)}, f32[8]{0:T(128)}, u32[]{:S(2)}) copy-start(f32[8]{0:T(128)} %get-tuple-element.85) | copy-start | bytes 100
  175.9 29.9 %copy-start.46 = (f32[8]{0:T(128)S(1)}, f32[8]{0:T(128)}, u32[]{:S(2)}) copy-start(f32[8]{0:T(128)} %get-tuple-element.86) | copy-start | bytes 100
  175.9 29.9 %copy-start.47 = (f32[8]{0:T(128)S(1)}, f32[8]{0:T(128)}, u32[]{:S(2)}) copy-start(f32[8]{0:T(128)} %get-tuple-element.87) | copy-start | bytes 100
  175.9 29.9 %copy-start.48 = (f32[8]{0:T(128)S(1)}, f32[8]{0:T(128)}, u32[]{:S(2)}) copy-start(f32[8]{0:T(128)} %get-tuple-element.88) | copy-start | bytes 100
  175.9 30.4 %copy-start.6 = (bf16[4,128,2,128]{3,1,2,0:T(8,128)(2,1)S(1)}, bf16[4,128,2,128]{3,1,2,0:T(8,128)(2,1)}, u32[]{:S(2)}) copy-start(bf16[4,128,2,128]{3,1,2,0:T(8,128)(2,1)} %copy.78) | copy-start | bytes 786436
  175.9 30.4 %copy-start.8 = (bf16[4,128,2,128]{3,1,2,0:T(8,128)(2,1)S(1)}, bf16[4,128,2,128]{3,1,2,0:T(8,128)(2,1)}, u32[]{:S(2)}) copy-start(bf16[4,128,2,128]{3,1,2,0:T(8,128)(2,1)} %copy-done.7) | copy-start | bytes 786436
  224.0 12.9 %all-to-all-start.1 = ((bf16[2,256,512]{1,2,0:T(8,128)(2,1)}), bf16[2,256,512]{1,2,0:T(8,128)(2,1)S(1)}, u32[]{:S(2)}, u32[]{:S(2)}) async-start(bf16[2,256,512]{1,2,0:T(8,128)(2,1)} %copy.88), calls=%async_computation.1 | async-start | bytes 1048576 | tf_op jit(solution)/shard_map/all_to_all | solution.py:477
  (31 other events, 45.1 us)
Sparse Core Ops, SparseCore 0:
  34.8 24.3 all-gather.6

commit v2 on v1

v2 whole, which is shorter than its diff:
```python
import jax
import jax.numpy as jnp
from jax import lax
from jax.experimental import pallas as pl
from jax.experimental.pallas import tpu as pltpu
from jax.sharding import Mesh
from jax.sharding import PartitionSpec as P

D = 2048
QK_DIM = 128
SSM_P = 64
STATE = 128
BLOCK = 128
ROWS = 512
HALF = 256
PAIR = 256
FS_SP = ("fs", "sp_0", "sp_1")
FS_SP_TP = ("fs", "sp_0", "sp_1", "tp")
MESH = pl.DeviceIdType.MESH
ORDER = (0, 1, 3, 2)
SCALE2 = QK_DIM ** (-0.5) * 1.4426950408889634
EPS = 1e-06
NEG = -1e30
F32, BF16 = jnp.float32, jnp.bfloat16


def matmul(a, b):
    return jnp.dot(a, b, preferred_element_type=F32)


def contract(a, b, da, db):
    return lax.dot_general(a, b, (((da,), (db,)), ((), ())), preferred_element_type=F32)


def arrived(ref, sem):
    pltpu.make_async_copy(ref, ref, sem).wait()


def layer_kernel(
    hidden,
    in_gain,
    w_query,
    w_key,
    w_value,
    w_gate,
    w_inner,
    w_bvec,
    w_cvec,
    w_step,
    conv_inner,
    conv_bvec,
    conv_cvec,
    a_log,
    decay_add,
    lambdas,
    head_gain,
    ssm_gain,
    out_attn,
    out_ssm,
    out_ref,
    x,
    normed,
    wq,
    wk,
    wv,
    wg,
    wx,
    wb,
    wc,
    ws,
    wo,
    kv_in,
    q_in,
    kv,
    q,
    acc,
    peak,
    total,
    done_out,
    back,
    pre,
    halo_out,
    halo_in,
    act,
    gate,
    narrow,
    cols,
    ysum,
    state,
    st_out,
    tot_out,
    st_y,
    tot_y,
    row_out,
    rtot_out,
    st_z,
    tot_z,
    ssm_all,
    ssm_buf,
    joined,
    lam_own,
    lam_in,
    load_sem,
    x_sem,
    wo_sem,
    zs_send,
    zs_recv,
    zq_send,
    zq_recv,
    ring_send,
    kv_recv,
    core_send,
    back_send,
    back_recv,
    halo_sem,
    sty_send,
    sty_recv,
    stz_send,
    stz_recv,
    ssm_sem,
    lam_sem,
):
    z, y, c = lax.axis_index("sp_0"), lax.axis_index("sp_1"), lax.axis_index("tp")
    right, left = lax.rem(y + 1, 4), lax.rem(y + 3, 4)
    other = 1 - c
    next_z = lax.rem(z + jnp.where(y == 3, 1, 0), 4)
    prev_z = lax.rem(z + jnp.where(y == 0, 3, 0), 4)

    loads = []
    for k, (src, dst) in enumerate(
        (
            (hidden, x.at[c]),
            (w_key, wk),
            (w_value, wv),
            (w_query, wq),
            (w_inner, wx),
            (w_bvec, wb),
            (w_cvec, wc),
            (w_gate, wg),
            (w_step, ws),
            (out_ssm, wo.at[c, 1]),
            (out_attn, wo.at[c, 0]),
        )
    ):
        loads.append(pltpu.make_async_copy(src, dst, load_sem.at[k]))
        loads[-1].start()

    barrier = pltpu.get_barrier_semaphore()

    def greet(where):
        pl.semaphore_signal(barrier, inc=1, device_id=where, device_id_type=MESH)

    for dz in range(4):
        for dc in range(2):
            if dz or dc:
                greet({"sp_0": lax.rem(z + dz, 4), "tp": lax.rem(c + dc, 2)})
    for dy in range(1, 4):
        greet({"sp_1": lax.rem(y + dy, 4)})
    greet({"sp_0": next_z, "sp_1": right})
    greet({"sp_0": prev_z, "sp_1": left})
    pl.semaphore_wait(barrier, 12)

    def remote(src, dst, send, recv, where):
        return pltpu.make_async_remote_copy(
            src_ref=src,
            dst_ref=dst,
            send_sem=send,
            recv_sem=recv,
            device_id=where,
            device_id_type=MESH,
        )

    x_copy = remote(hidden, x.at[c], x_sem.at[0], x_sem.at[1], {"tp": other})
    x_copy.start()

    acc[...] = jnp.zeros_like(acc)
    total[...] = jnp.zeros_like(total)
    peak[...] = jnp.full_like(peak, NEG)
    narrow[...] = jnp.zeros_like(narrow)
    for i in range(2):
        lam_own[i] = jnp.full((8, 128), lambdas[0, i], F32)
    lam_copy = remote(lam_own, lam_in, lam_sem.at[0], lam_sem.at[1], {"tp": other})
    lam_copy.start()

    loads[0].wait()
    arrived(x.at[other], x_sem.at[1])

    def norm_rows(n, carry):
        rows = pl.ds(pl.multiple_of(n * 64, 64), 64)
        first, second = x[0, rows, :].astype(F32), x[1, rows, :].astype(F32)
        squares = jnp.sum(first * first, axis=1, keepdims=True) + jnp.sum(
            second * second, axis=1, keepdims=True
        )
        scale = lax.rsqrt(squares / D + EPS)
        normed[rows, 0:1024] = (first * scale * in_gain[:, 0:1024]).astype(BF16)
        normed[rows, 1024:2048] = (second * scale * in_gain[:, 1024:2048]).astype(BF16)
        return carry

    lax.fori_loop(0, 8, norm_rows, 0)

    wo_copies = [
        remote(out_ssm, wo.at[c, 1], wo_sem.at[0], wo_sem.at[1], {"tp": other}),
        remote(out_attn, wo.at[c, 0], wo_sem.at[2], wo_sem.at[3], {"tp": other}),
    ]

    def exchange(src, dst, send, recv, j):
        to, r = 2 * c + j // 2, j % 2
        mine = jnp.logical_and(to == z, c == r)

        @pl.when(mine)
        def _():
            pltpu.make_async_copy(src.at[j], dst, recv.at[z]).start()

        @pl.when(jnp.logical_not(mine))
        def _():
            remote(src.at[j], dst, send.at[j], recv.at[z], {"sp_0": to, "tp": r}).start()

    loads[1].wait()
    loads[2].wait()
    for i in range(2):
        lanes = slice(i * PAIR, (i + 1) * PAIR)
        keys = matmul(normed[...], wk[:, lanes])
        for r in range(2):
            kv_in[2 * i + r, 0] = keys[r * HALF : (r + 1) * HALF].astype(BF16)
        values = matmul(normed[...], wv[:, lanes])
        for r in range(2):
            kv_in[2 * i + r, 1] = values[r * HALF : (r + 1) * HALF].T.astype(BF16)
        for r in range(2):
            exchange(kv_in, kv.at[0, z], zs_send, zs_recv, 2 * i + r)
    for copy in wo_copies:
        copy.start()
    loads[3].wait()
    for i in range(2):
        queries = matmul(normed[...], wq[:, i * PAIR : (i + 1) * PAIR])
        for r in range(2):
            q_in[2 * i + r] = queries[r * HALF : (r + 1) * HALF].T.astype(BF16)
            exchange(q_in, q.at[z], zq_send, zq_recv, 2 * i + r)

    def to_neighbour(slot, zz, new_slot, yy, k):
        return remote(
            kv.at[slot, zz],
            kv.at[new_slot, zz],
            ring_send.at[k],
            kv_recv.at[new_slot, zz],
            {"sp_1": yy},
        )

    def to_partner(slot, zz):
        return remote(
            kv.at[slot, zz],
            kv.at[slot + 1, zz],
            core_send.at[slot // 2, zz],
            kv_recv.at[slot + 1, zz],
            {"tp": other},
        )

    at = [lax.rem(z + d, 4) for d in ORDER]

    def serve(t):
        arrived(kv.at[0, at[t]], zs_recv.at[at[t]])
        to_neighbour(0, at[t], 6, right, t).start()
        to_neighbour(0, at[t], 2, left, 4 + t).start()
        to_partner(0, at[t]).start()

    serve(0)

    for k in (4, 5, 6):
        loads[k].wait()
    for wide, lanes, at_lane in (
        (wx, slice(0, 256), 0),
        (wx, slice(256, 512), 256),
        (wb, slice(0, 256), 512),
        (wc, slice(0, 256), 768),
    ):
        part = matmul(normed[...], wide[:, lanes]).astype(BF16)
        pre[8:520, at_lane : at_lane + 256] = part.astype(F32)
        halo_out[:, at_lane : at_lane + 256] = part[496:512]
    halo_copy = remote(
        halo_out, halo_in, halo_sem.at[0], halo_sem.at[1], {"sp_0": next_z, "sp_1": right}
    )
    halo_copy.start()
    loads[7].wait()
    for i in range(2):
        lanes = slice(i * 256, (i + 1) * 256)
        gate[:, lanes] = matmul(normed[...], wg[:, lanes]).astype(BF16)
    loads[8].wait()
    narrow[0, :, 0:8] = matmul(normed[...], ws[...]).astype(BF16).astype(F32)
    narrow[1, :, 0:8] = decay_add[...]
    arrived(halo_in, halo_sem.at[1])
    begins = jnp.logical_and(z == 0, y == 0)
    pre[0:8, :] = halo_in[...].astype(F32)[8:16] * jnp.where(begins, 0.0, 1.0)
    for at_lane, (taps, lanes) in enumerate(
        (
            (conv_inner, slice(0, 256)),
            (conv_inner, slice(256, 512)),
            (conv_bvec, slice(0, 256)),
            (conv_cvec, slice(0, 256)),
        )
    ):
        here = slice(at_lane * 256, at_lane * 256 + 256)
        weight = taps[:, lanes].astype(F32)
        for n in range(4):
            summed = pre[5 + n * BLOCK : 5 + (n + 1) * BLOCK, here] * weight[0:1]
            for o in range(1, 4):
                summed = (
                    summed + pre[5 + o + n * BLOCK : 5 + o + (n + 1) * BLOCK, here] * weight[o : o + 1]
                )
            act[n * BLOCK : (n + 1) * BLOCK, here] = (summed * jax.nn.sigmoid(summed)).astype(BF16)

    serve(1)

    rate = jnp.zeros((8, 128), F32)
    sub = lax.broadcasted_iota(jnp.int32, (8, 128), 0)
    lane8 = lax.broadcasted_iota(jnp.int32, (8, 128), 1)
    for h in range(8):
        rate = jnp.where(sub == h, a_log[0, h], rate)
    rate = -jnp.exp(rate)
    t_at = lax.broadcasted_iota(jnp.int32, (BLOCK, BLOCK), 0)
    s_at = lax.broadcasted_iota(jnp.int32, (BLOCK, BLOCK), 1)
    causal = s_at <= t_at
    low_lane = s_at < SSM_P
    quarter = lax.broadcasted_iota(jnp.int32, (BLOCK, 256), 1) // SSM_P

    def spread(tile, first):
        pairs = [
            jnp.where(low_lane, tile[:, first + a : first + a + 1], tile[:, first + a + 1 : first + a + 2])
            for a in (0, 2)
        ]
        return jnp.concatenate(pairs, axis=1)

    def by_head(tile):
        return jnp.concatenate(
            [jnp.broadcast_to(tile[h : h + 1], (SSM_P, 128)) for h in range(tile.shape[0])], axis=0
        )

    def split_dot(left_side, right_side):
        high = right_side.astype(BF16)
        low = (right_side - high.astype(F32)).astype(BF16)
        return contract(left_side, high, 1, 1) + contract(left_side, low, 1, 1)

    state[...] = jnp.zeros_like(state)
    preceding = jnp.zeros((8, 128), F32)
    for n in range(4):
        rows = slice(n * BLOCK, (n + 1) * BLOCK)
        step_pre = narrow[0, rows, :].T[0:8]
        decay_row = narrow[1, rows, :].T[0:8]
        size = jnp.maximum(step_pre, 0.0) + jnp.log1p(jnp.exp(-jnp.abs(step_pre)))
        running = rate * size + decay_row
        for shift in (1, 2, 4, 8, 16, 32, 64):
            running = running + jnp.where(lane8 >= shift, pltpu.roll(running, shift, 1), 0.0)
        last = jnp.broadcast_to(running[:, 127:128], (8, 128))
        to_end = jnp.exp(last - running) * size
        tall = jnp.concatenate(
            [running, to_end, jnp.exp(running), jnp.exp(running + preceding), jnp.zeros((96, 128), F32)],
            axis=0,
        ).T
        cols[rows, :] = tall
        keep = jnp.exp(last)
        preceding = preceding + last
        for g in range(2):
            lanes = slice(g * 256, (g + 1) * 256)
            inputs_x = act[rows, lanes]
            inputs_b = act[rows, 512 + g * 128 : 640 + g * 128]
            inputs_c = act[rows, 768 + g * 128 : 896 + g * 128]
            crossing = contract(inputs_c, inputs_b, 1, 1)
            mixes, own_x = [], []
            for a in range(4):
                h = 4 * g + a
                fade = jnp.exp(
                    jnp.where(causal, tall[:, h : h + 1] - running[h : h + 1, :], NEG)
                )
                mixes.append((crossing * fade * size[h : h + 1, :]).astype(BF16))
                own_x.append(jnp.where(quarter == a, inputs_x, jnp.zeros_like(inputs_x)))
            inside = matmul(jnp.concatenate(mixes, axis=1), jnp.concatenate(own_x, axis=0))
            weighted = (inputs_x.astype(F32) * spread(tall, 8 + 4 * g)).astype(BF16)
            fresh = contract(weighted, inputs_b, 0, 0)
            before = state[lanes, :]
            carried = split_dot(inputs_c, before) * spread(tall, 16 + 4 * g)
            ysum[rows, lanes] = inside + carried
            state[lanes, :] = before * by_head(keep[4 * g : 4 * g + 4]) + fresh
    st_out[...] = state[...].astype(BF16)
    tot_out[...] = preceding
    st_y[y] = state[...].astype(BF16)
    tot_y[y] = preceding
    for dy in range(1, 4):
        where = {"sp_1": lax.rem(y + dy, 4)}
        remote(st_out, st_y.at[y], sty_send.at[0, dy], sty_recv.at[0, y], where).start()
        remote(tot_out, tot_y.at[y], sty_send.at[1, dy], sty_recv.at[1, y], where).start()

    serve(2)
    serve(3)

    def wait_chunk(slot, zz):
        arrived(kv.at[slot, zz], kv_recv.at[slot, zz])

    own = 2 * y + c

    def block(zq, slot, zc, masked):
        for m in range(2):
            lanes = slice(m * QK_DIM, (m + 1) * QK_DIM)
            scores = matmul(kv[slot, zc, 0, :, lanes], q[zq, lanes, :]) * SCALE2
            if masked:
                key_at = lax.broadcasted_iota(jnp.int32, scores.shape, 0)
                query_at = lax.broadcasted_iota(jnp.int32, scores.shape, 1)
                scores = jnp.where(key_at <= query_at, scores, NEG)
            old = peak[zq, m]
            new = jnp.maximum(old, jnp.max(scores, axis=0, keepdims=True))
            weights = jnp.exp2(scores - new[0:1])
            shrink = jnp.exp2(old - new)
            peak[zq, m] = new
            total[zq, m] = total[zq, m] * shrink + jnp.sum(weights, axis=0, keepdims=True)
            acc[zq, m] = acc[zq, m] * shrink[0:1] + matmul(kv[slot, zc, 1], weights.astype(BF16))

    def over(slot, t):
        zc = at[t]
        if slot == 0:
            block(zc, slot, zc, True)
            low = zc + 1
        else:
            theirs = 2 * lax.rem(y + slot // 2, 4) + (c if slot % 2 == 0 else other)
            low = zc + jnp.where(theirs > own, 1, 0)

        def step(zq, carry):
            block(zq, slot, zc, False)
            return carry

        lax.fori_loop(low, 4, step, 0)

    def prefix(states, totals, mine, send_states, send_totals):
        run_s, run_t = jnp.zeros((512, 128), F32), jnp.zeros((8, 128), F32)
        before_s, before_t = run_s, run_t
        for k in range(4):
            run_s = run_s * by_head(jnp.exp(totals[k])) + states[k].astype(F32)
            run_t = run_t + totals[k]
            before_s = jnp.where(k < mine, run_s, before_s)
            before_t = jnp.where(k < mine, run_t, before_t)
        if send_states is not None:
            send_states[...] = run_s.astype(BF16)
            send_totals[...] = run_t
            st_z[z] = run_s.astype(BF16)
            tot_z[z] = run_t
        return before_s, before_t

    for t in range(4):
        arrived(q.at[at[t]], zq_recv.at[at[t]])
    for t in range(4):
        over(0, t)
    for dy in range(1, 4):
        yy = lax.rem(y + dy, 4)
        arrived(st_y.at[yy], sty_recv.at[0, yy])
        arrived(tot_y.at[yy], sty_recv.at[1, yy])
    row_before, row_total = prefix(st_y, tot_y, y, row_out, rtot_out)
    state[...] = row_before
    tot_out2 = row_total
    for dz in range(1, 4):
        where = {"sp_0": lax.rem(z + dz, 4)}
        remote(row_out, st_z.at[z], stz_send.at[0, dz], stz_recv.at[0, z], where).start()
        remote(rtot_out, tot_z.at[z], stz_send.at[1, dz], stz_recv.at[1, z], where).start()
    for t in range(4):
        wait_chunk(1, at[t])
        over(1, t)

    def finish_ssm():
        for dz in range(1, 4):
            zz = lax.rem(z + dz, 4)
            arrived(st_z.at[zz], stz_recv.at[0, zz])
            arrived(tot_z.at[zz], stz_recv.at[1, zz])
        far, _ = prefix(st_z, tot_z, z, None, None)
        state[...] = far * by_head(jnp.exp(tot_out2)) + state[...]
        for n in range(4):
            rows = slice(n * BLOCK, (n + 1) * BLOCK)
            for g in range(2):
                lanes = slice(g * 256, (g + 1) * 256)
                inputs_c = act[rows, 768 + g * 128 : 896 + g * 128]
                value = ysum[rows, lanes] + split_dot(inputs_c, state[lanes, :]) * spread(
                    cols[rows, :], 24 + 4 * g
                )
                opened = gate[rows, lanes].astype(F32)
                value = value * (opened * jax.nn.sigmoid(opened))
                scale = lax.rsqrt(jnp.mean(value * value, axis=1, keepdims=True) + EPS)
                ssm_all[n // 2, (n % 2) * BLOCK : (n % 2 + 1) * BLOCK, lanes] = (
                    value * scale * ssm_gain[:, lanes]
                ).astype(BF16)
        ssm_buf[c] = ssm_all[c]
        remote(ssm_all.at[other], ssm_buf.at[c], ssm_sem.at[0], ssm_sem.at[1], {"tp": other}).start()

    def project_ssm():
        arrived(ssm_buf.at[other], ssm_sem.at[1])
        loads[9].wait()
        arrived(wo.at[other, 1], wo_sem.at[1])
        for k in range(4):
            lanes = slice(k * 512, (k + 1) * 512)
            joined[:, lanes] = matmul(ssm_buf[0], wo[0, 1, :, lanes]) + matmul(
                ssm_buf[1], wo[1, 1, :, lanes]
            )

    for t in range(4):
        wait_chunk(6, at[t])
        if t < 2:
            to_neighbour(6, at[t], 4, right, 8 + t).start()
        to_partner(6, at[t]).start()
        wait_chunk(2, at[t])
        if t >= 2:
            to_neighbour(2, at[t], 4, left, 8 + t).start()
        to_partner(2, at[t]).start()
        over(6, t)
        over(2, t)
        if t:
            wait_chunk(7, at[t - 1])
            over(7, t - 1)
            wait_chunk(3, at[t - 1])
            over(3, t - 1)
        if t == 0:
            finish_ssm()
        if t == 1:
            project_ssm()
    wait_chunk(7, at[3])
    over(7, 3)
    wait_chunk(3, at[3])
    over(3, 3)
    for t in (0, 2, 1, 3):
        wait_chunk(4, at[t])
        to_partner(4, at[t]).start()
        over(4, t)
    for t in (0, 2, 1, 3):
        wait_chunk(5, at[t])
        over(5, t)

    arrived(lam_in, lam_sem.at[1])
    held = jnp.where(z // 2 == c, lam_own[lax.rem(z, 2)], lam_in[lax.rem(z, 2)])
    lam = jnp.concatenate([held, held], axis=1)[0:1]
    gain_col = jnp.broadcast_to(head_gain[...], (PAIR, PAIR)).T
    for dz in ORDER:
        zz = lax.rem(z + dz, 4)
        differ = acc[zz, 0] / total[zz, 0, 0:1] - lam * (acc[zz, 1] / total[zz, 1, 0:1])
        scale = lax.rsqrt(jnp.mean(differ * differ, axis=0, keepdims=True) + EPS)
        done_out[zz] = (differ * scale * gain_col).astype(BF16)
        if dz == 0:
            back[zz] = done_out[zz]
        else:
            remote(
                done_out.at[zz], back.at[z], back_send.at[dz], back_recv.at[z], {"sp_0": zz}
            ).start()
    loads[10].wait()
    arrived(wo.at[other, 0], wo_sem.at[3])
    for dz in range(1, 4):
        zz = lax.rem(z + dz, 4)
        arrived(back.at[zz], back_recv.at[zz])
    for k in range(4):
        lanes = slice(k * 512, (k + 1) * 512)
        sum_k = joined[:, lanes]
        for h in range(4):
            sum_k = sum_k + contract(
                back[h], wo[h // 2, 0, (h % 2) * PAIR : (h % 2 + 1) * PAIR, lanes], 0, 0
            )
        out_ref[:, lanes] = sum_k.astype(BF16)

    x_copy.wait_send()
    lam_copy.wait_send()
    halo_copy.wait_send()
    for copy in wo_copies:
        copy.wait_send()
    for j in range(4):
        mine = jnp.logical_and(2 * c + j // 2 == z, c == j % 2)

        @pl.when(jnp.logical_not(mine))
        def _():
            arrived(kv_in.at[j], zs_send.at[j])
            arrived(q_in.at[j], zq_send.at[j])

    for k in range(12):
        arrived(kv.at[0, 0], ring_send.at[k])
    for s in range(4):
        for t in range(4):
            arrived(kv.at[0, 0], core_send.at[s, t])
    for d in range(1, 4):
        arrived(done_out.at[0], back_send.at[d])
        arrived(st_out, sty_send.at[0, d])
        arrived(tot_out, sty_send.at[1, d])
        arrived(row_out, stz_send.at[0, d])
        arrived(rtot_out, stz_send.at[1, d])
    arrived(ssm_all.at[0], ssm_sem.at[0])


def per_device(
    hidden_in,
    in_gain,
    w_query,
    w_key,
    w_value,
    w_gate,
    w_inner,
    w_bvec,
    w_cvec,
    w_step,
    conv_inner,
    conv_bvec,
    conv_cvec,
    a_log,
    decay_add,
    lambdas,
    head_gain,
    ssm_gain,
    out_attn,
    out_ssm,
):
    vmem = pl.BlockSpec(memory_space=pltpu.VMEM)
    smem = pl.BlockSpec(memory_space=pltpu.SMEM)
    away = pl.BlockSpec(memory_space=pl.ANY)
    dma = pltpu.SemaphoreType.DMA
    buf = pltpu.VMEM
    return pl.pallas_call(
        layer_kernel,
        out_shape=jax.ShapeDtypeStruct((HALF, D), BF16),
        in_specs=[away, vmem]
        + [away] * 8
        + [vmem] * 3
        + [smem, vmem, smem, vmem, vmem, away, away],
        out_specs=vmem,
        scratch_shapes=[
            buf((2, ROWS, 1024), BF16),
            buf((ROWS, D), BF16),
            buf((D, 512), BF16),
            buf((D, 512), BF16),
            buf((D, 512), BF16),
            buf((D, 512), BF16),
            buf((D, 512), BF16),
            buf((D, 256), BF16),
            buf((D, 256), BF16),
            buf((D, 8), BF16),
            buf((2, 2, 512, D), BF16),
            buf((4, 2, HALF, PAIR), BF16),
            buf((4, PAIR, HALF), BF16),
            buf((8, 4, 2, HALF, PAIR), BF16),
            buf((4, PAIR, HALF), BF16),
            buf((4, 2, PAIR, HALF), F32),
            buf((4, 2, 8, HALF), F32),
            buf((4, 2, 8, HALF), F32),
            buf((4, PAIR, HALF), BF16),
            buf((4, PAIR, HALF), BF16),
            buf((520, 1024), F32),
            buf((16, 1024), BF16),
            buf((16, 1024), BF16),
            buf((ROWS, 1024), BF16),
            buf((ROWS, 512), BF16),
            buf((2, ROWS, 128), F32),
            buf((ROWS, 128), F32),
            buf((ROWS, 512), F32),
            buf((512, 128), F32),
            buf((512, 128), BF16),
            buf((8, 128), F32),
            buf((4, 512, 128), BF16),
            buf((4, 8, 128), F32),
            buf((512, 128), BF16),
            buf((8, 128), F32),
            buf((4, 512, 128), BF16),
            buf((4, 8, 128), F32),
            buf((2, HALF, 512), BF16),
            buf((2, HALF, 512), BF16),
            buf((HALF, D), F32),
            buf((2, 8, 128), F32),
            buf((2, 8, 128), F32),
            dma((11,)),
            dma((2,)),
            dma((4,)),
            dma((4,)),
            dma((4,)),
            dma((4,)),
            dma((4,)),
            dma((12,)),
            dma((8, 4)),
            dma((4, 4)),
            dma((4,)),
            dma((4,)),
            dma((2,)),
            dma((2, 4)),
            dma((2, 4)),
            dma((2, 4)),
            dma((2, 4)),
            dma((2,)),
            dma((2,)),
        ],
        compiler_params=pltpu.CompilerParams(
            collective_id=0, has_side_effects=True, vmem_limit_bytes=63 * 2**20
        ),
    )(
        hidden_in,
        in_gain.reshape(1, D),
        w_query,
        w_key,
        w_value,
        w_gate,
        w_inner,
        w_bvec,
        w_cvec,
        w_step,
        conv_inner,
        conv_bvec,
        conv_cvec,
        a_log.reshape(1, 8),
        decay_add,
        lambdas.reshape(1, 2),
        head_gain.reshape(1, PAIR),
        ssm_gain.reshape(1, 512),
        out_attn,
        out_ssm,
    )


def solution(mesh):
    split = Mesh(
        mesh.devices.reshape(4, 4, mesh.shape["fs"], mesh.shape["tp"]), ("sp_0", "sp_1", "fs", "tp")
    )
    in_specs = (
        P(FS_SP, "tp"),
        P(),
        P(None, "tp"),
        P(None, "tp"),
        P(None, "tp"),
        P(None, "tp"),
        P(None, "tp"),
        P(None, "tp"),
        P(None, "tp"),
        P(None, "tp"),
        P(None, "tp"),
        P(None, "tp"),
        P(None, "tp"),
        P("tp"),
        P(FS_SP, "tp"),
        P("tp"),
        P(),
        P("tp"),
        P("tp", None),
        P("tp", None),
    )
    out_specs = P(FS_SP_TP, None)
    return jax.shard_map(
        per_device, mesh=split, in_specs=in_specs, out_specs=out_specs, check_vma=False
    )
```

time: 254 us -> 98 us (0.39)
  the two profiles are of different devices: /device:TPU:1 before, /device:TPU:31 now
where the time goes in v2:
time: 98 us; the launch traced here: 97.7 us
  Pallas kernels  92 us (94%)
  local copies, waits for them, and re-layouts  5.63 us (6%)
    pallas_call x1, Pallas kernels, per_device(): pl.pallas_call(layer_kernel, out_shape=jax.ShapeDtypeStruct((HALF, D), BF...  92 us
    unnamed x3, local copies, waits for them, and re-layouts  5.63 us

profile of v2, /device:TPU:31, one launch (start us, length us, event | category | flops | bytes accessed | tf_op | source)
XLA Modules:
  0.0 97.7 jit_solution(15421101007467104840)
XLA Ops:
  0.0 1.6 %copy.22.decay_add = f32[512,8]{1,0:T(8,128)} copy(f32[512,8]{0,1:T(8,128)} %param.34) | data formatting | bytes 32768 | tf_op args[14]
  1.6 1.8 %copy.21.w_step = bf16[2048,8]{1,0:T(8,128)(2,1)} copy(bf16[2048,8]{0,1:T(8,128)(2,1)} %param.29) | data formatting | bytes 65536 | tf_op args[9]
  3.3 92.0 %shard_map.190 = bf16[256,2048]{1,0:T(8,128)(2,1)} custom-call(bf16[512,1024]{1,0:T(8,128)(2,1)} %hidden.1, f32[1,2048]{1,0:T(1,128)} %bitcast.5, bf16[2048,512]{1,0:T(8,128)(2,1)} %w_query.1, bf16[2048,512]{1,0:T(8,128)(2,1)} %w_key.1, bf16[2048,512]{1,0:T(8,128)(2,1)} %w_value.1, bf16[2048,512]{1,0:T(8,128)(2,1)} %w_gate.1, bf16[2048,512]{1,0:T(8,128)(2,1)} %w_inner.1, ...), custom_call_target="tpu_custom_call" | custom-call | tf_op jit(solution)/shard_map/pallas_call | solution.py:612
  95.4 2.3 %copy.24 = bf16[256,2048]{1,0:T(8,128)(2,1)} copy(bf16[256,2048]{1,0:T(8,128)(2,1)} %shard_map.190) | data formatting | bytes 2097152

commit v3 on v2

--- a/solution.py
+++ b/solution.py
@@ -17,7 +17,6 @@
 FS_SP = ("fs", "sp_0", "sp_1")
 FS_SP_TP = ("fs", "sp_0", "sp_1", "tp")
 MESH = pl.DeviceIdType.MESH
-ORDER = (0, 1, 3, 2)
 SCALE2 = QK_DIM ** (-0.5) * 1.4426950408889634
 EPS = 1e-06
 NEG = -1e30
@@ -95,11 +94,17 @@
     rtot_out,
     st_z,
     tot_z,
+    pre_s,
+    pre_t,
+    inc_out,
+    inc_in,
     ssm_all,
     ssm_buf,
     joined,
     lam_own,
     lam_in,
+    gain_col,
+    result,
     load_sem,
     x_sem,
     wo_sem,
@@ -119,6 +124,9 @@
     stz_recv,
     ssm_sem,
     lam_sem,
+    out_sem,
+    inc_send,
+    inc_recv,
 ):
     z, y, c = lax.axis_index("sp_0"), lax.axis_index("sp_1"), lax.axis_index("tp")
     right, left = lax.rem(y + 1, 4), lax.rem(y + 3, 4)
@@ -176,7 +184,6 @@
     acc[...] = jnp.zeros_like(acc)
     total[...] = jnp.zeros_like(total)
     peak[...] = jnp.full_like(peak, NEG)
-    narrow[...] = jnp.zeros_like(narrow)
     for i in range(2):
         lam_own[i] = jnp.full((8, 128), lambdas[0, i], F32)
     lam_copy = remote(lam_own, lam_in, lam_sem.at[0], lam_sem.at[1], {"tp": other})
@@ -229,13 +236,6 @@
             exchange(kv_in, kv.at[0, z], zs_send, zs_recv, 2 * i + r)
     for copy in wo_copies:
         copy.start()
-    loads[3].wait()
-    for i in range(2):
-        queries = matmul(normed[...], wq[:, i * PAIR : (i + 1) * PAIR])
-        for r in range(2):
-            q_in[2 * i + r] = queries[r * HALF : (r + 1) * HALF].T.astype(BF16)
-            exchange(q_in, q.at[z], zq_send, zq_recv, 2 * i + r)
-
     def to_neighbour(slot, zz, new_slot, yy, k):
         return remote(
             kv.at[slot, zz],
@@ -254,7 +254,7 @@
             {"tp": other},
         )
 
-    at = [lax.rem(z + d, 4) for d in ORDER]
+    at = [z, lax.rem(z + 1, 2), jnp.where(z < 2, 2, z - 2), jnp.where(z == 3, 2, 3)]
 
     def serve(t):
         arrived(kv.at[0, at[t]], zs_recv.at[at[t]])
@@ -262,7 +262,15 @@
         to_neighbour(0, at[t], 2, left, 4 + t).start()
         to_partner(0, at[t]).start()
 
-    serve(0)
+    loads[3].wait()
+    for i in range(2):
+        if i:
+            serve(0)
+        queries = matmul(normed[...], wq[:, i * PAIR : (i + 1) * PAIR])
+        for r in range(2):
+            q_in[2 * i + r] = queries[r * HALF : (r + 1) * HALF].T.astype(BF16)
+            exchange(q_in, q.at[z], zq_send, zq_recv, 2 * i + r)
+
 
     for k in (4, 5, 6):
         loads[k].wait()
@@ -284,30 +292,33 @@
         lanes = slice(i * 256, (i + 1) * 256)
         gate[:, lanes] = matmul(normed[...], wg[:, lanes]).astype(BF16)
     loads[8].wait()
-    narrow[0, :, 0:8] = matmul(normed[...], ws[...]).astype(BF16).astype(F32)
-    narrow[1, :, 0:8] = decay_add[...]
+    narrow[...] = contract(ws[...], normed[...], 1, 1).astype(BF16).astype(F32)
+
+    def convolve(blocks):
+        for at_lane, (taps, lanes) in enumerate(
+            (
+                (conv_inner, slice(0, 256)),
+                (conv_inner, slice(256, 512)),
+                (conv_bvec, slice(0, 256)),
+                (conv_cvec, slice(0, 256)),
+            )
+        ):
+            here = slice(at_lane * 256, at_lane * 256 + 256)
+            weight = taps[:, lanes].astype(F32)
+            for n in blocks:
+                first = 5 + n * BLOCK
+                summed = pre[first : first + BLOCK, here] * weight[0:1]
+                for o in range(1, 4):
+                    summed = summed + pre[first + o : first + o + BLOCK, here] * weight[o : o + 1]
+                act[n * BLOCK : (n + 1) * BLOCK, here] = (
+                    summed * jax.nn.sigmoid(summed)
+                ).astype(BF16)
+
+    convolve((1, 2, 3))
     arrived(halo_in, halo_sem.at[1])
     begins = jnp.logical_and(z == 0, y == 0)
     pre[0:8, :] = halo_in[...].astype(F32)[8:16] * jnp.where(begins, 0.0, 1.0)
-    for at_lane, (taps, lanes) in enumerate(
-        (
-            (conv_inner, slice(0, 256)),
-            (conv_inner, slice(256, 512)),
-            (conv_bvec, slice(0, 256)),
-            (conv_cvec, slice(0, 256)),
-        )
-    ):
-        here = slice(at_lane * 256, at_lane * 256 + 256)
-        weight = taps[:, lanes].astype(F32)
-        for n in range(4):
-            summed = pre[5 + n * BLOCK : 5 + (n + 1) * BLOCK, here] * weight[0:1]
-            for o in range(1, 4):
-                summed = (
-                    summed + pre[5 + o + n * BLOCK : 5 + o + (n + 1) * BLOCK, here] * weight[o : o + 1]
-                )
-            act[n * BLOCK : (n + 1) * BLOCK, here] = (summed * jax.nn.sigmoid(summed)).astype(BF16)
-
-    serve(1)
+    convolve((0,))
 
     rate = jnp.zeros((8, 128), F32)
     sub = lax.broadcasted_iota(jnp.int32, (8, 128), 0)
@@ -342,8 +353,8 @@
     preceding = jnp.zeros((8, 128), F32)
     for n in range(4):
         rows = slice(n * BLOCK, (n + 1) * BLOCK)
-        step_pre = narrow[0, rows, :].T[0:8]
-        decay_row = narrow[1, rows, :].T[0:8]
+        step_pre = narrow[:, rows]
+        decay_row = decay_add[:, rows]
         size = jnp.maximum(step_pre, 0.0) + jnp.log1p(jnp.exp(-jnp.abs(step_pre)))
         running = rate * size + decay_row
         for shift in (1, 2, 4, 8, 16, 32, 64):
@@ -378,14 +389,19 @@
             carried = split_dot(inputs_c, before) * spread(tall, 16 + 4 * g)
             ysum[rows, lanes] = inside + carried
             state[lanes, :] = before * by_head(keep[4 * g : 4 * g + 4]) + fresh
-    st_out[...] = state[...].astype(BF16)
-    tot_out[...] = preceding
-    st_y[y] = state[...].astype(BF16)
-    tot_y[y] = preceding
+        if n == 0:
+            serve(1)
+    for j in range(4):
+        st_out[j] = state[j * 128 : (j + 1) * 128, :].astype(BF16)
+        tot_out[j] = jnp.concatenate(
+            [jnp.broadcast_to(preceding[2 * j + e : 2 * j + e + 1], (4, 128)) for e in range(2)], axis=0
+        )
+    st_y[y] = st_out[y]
+    tot_y[y] = tot_out[y]
     for dy in range(1, 4):
-        where = {"sp_1": lax.rem(y + dy, 4)}
-        remote(st_out, st_y.at[y], sty_send.at[0, dy], sty_recv.at[0, y], where).start()
-        remote(tot_out, tot_y.at[y], sty_send.at[1, dy], sty_recv.at[1, y], where).start()
+        yy = lax.rem(y + dy, 4)
+        remote(st_out.at[yy], st_y.at[y], sty_send.at[0, yy], sty_recv.at[0, y], {"sp_1": yy}).start()
+        remote(tot_out.at[yy], tot_y.at[y], sty_send.at[1, yy], sty_recv.at[1, y], {"sp_1": yy}).start()
 
     serve(2)
     serve(3)
@@ -393,86 +409,126 @@
     def wait_chunk(slot, zz):
         arrived(kv.at[slot, zz], kv_recv.at[slot, zz])
 
-    own = 2 * y + c
-
-    def block(zq, slot, zc, masked):
-        for m in range(2):
-            lanes = slice(m * QK_DIM, (m + 1) * QK_DIM)
-            scores = matmul(kv[slot, zc, 0, :, lanes], q[zq, lanes, :]) * SCALE2
-            if masked:
-                key_at = lax.broadcasted_iota(jnp.int32, scores.shape, 0)
-                query_at = lax.broadcasted_iota(jnp.int32, scores.shape, 1)
-                scores = jnp.where(key_at <= query_at, scores, NEG)
-            old = peak[zq, m]
-            new = jnp.maximum(old, jnp.max(scores, axis=0, keepdims=True))
-            weights = jnp.exp2(scores - new[0:1])
+    def unit(zqs, pair, zc, masked):
+        parts = []
+        for zq in zqs:
+            for m in range(2):
+                lanes = slice(m * QK_DIM, (m + 1) * QK_DIM)
+                queries = q[zq, lanes, :]
+                scores = [matmul(kv[2 * pair + e, zc, 0, :, lanes], queries) for e in range(2)]
+                if masked:
+                    key_at = lax.broadcasted_iota(jnp.int32, scores[0].shape, 0)
+                    query_at = lax.broadcasted_iota(jnp.int32, scores[0].shape, 1)
+                    scores = [
+                        jnp.where(key_at <= query_at, scores[0], NEG),
+                        jnp.where(key_at <= query_at + (2 * c - 1) * HALF, scores[1], NEG),
+                    ]
+                parts.append((zq, m, scores, peak[zq, m], total[zq, m]))
+        ready = []
+        for zq, m, scores, old, sums in parts:
+            top = jnp.maximum(
+                jnp.max(scores[0], axis=0, keepdims=True), jnp.max(scores[1], axis=0, keepdims=True)
+            )
+            new = jnp.maximum(old, top * SCALE2)
+            weights = [jnp.exp2(part * SCALE2 - new[0:1]) for part in scores]
             shrink = jnp.exp2(old - new)
+            sums = sums * shrink + (
+                jnp.sum(weights[0], axis=0, keepdims=True) + jnp.sum(weights[1], axis=0, keepdims=True)
+            )
+            value = matmul(kv[2 * pair, zc, 1], weights[0].astype(BF16)) + matmul(
+                kv[2 * pair + 1, zc, 1], weights[1].astype(BF16)
+            )
+            ready.append((zq, m, new, sums, acc[zq, m] * shrink[0:1] + value))
+        for zq, m, new, sums, value in ready:
             peak[zq, m] = new
-            total[zq, m] = total[zq, m] * shrink + jnp.sum(weights, axis=0, keepdims=True)
-            acc[zq, m] = acc[zq, m] * shrink[0:1] + matmul(kv[slot, zc, 1], weights.astype(BF16))
-
-    def over(slot, t):
-        zc = at[t]
-        if slot == 0:
-            block(zc, slot, zc, True)
-            low = zc + 1
-        else:
-            theirs = 2 * lax.rem(y + slot // 2, 4) + (c if slot % 2 == 0 else other)
-            low = zc + jnp.where(theirs > own, 1, 0)
-
-        def step(zq, carry):
-            block(zq, slot, zc, False)
+            total[zq, m] = sums
+            acc[zq, m] = value
+
+    def over(pair, zc, low):
+        def two(k, carry):
+            unit([3 - 2 * k, 2 - 2 * k], pair, zc, False)
             return carry
 
-        lax.fori_loop(low, 4, step, 0)
-
-    def prefix(states, totals, mine, send_states, send_totals):
-        run_s, run_t = jnp.zeros((512, 128), F32), jnp.zeros((8, 128), F32)
-        before_s, before_t = run_s, run_t
-        for k in range(4):
-            run_s = run_s * by_head(jnp.exp(totals[k])) + states[k].astype(F32)
-            run_t = run_t + totals[k]
-            before_s = jnp.where(k < mine, run_s, before_s)
-            before_t = jnp.where(k < mine, run_t, before_t)
-        if send_states is not None:
-            send_states[...] = run_s.astype(BF16)
-            send_totals[...] = run_t
-            st_z[z] = run_s.astype(BF16)
-            tot_z[z] = run_t
-        return before_s, before_t
-
+        lax.fori_loop(0, (4 - low) // 2, two, 0)
+
+        @pl.when(lax.rem(low, 2) == 1)
+        def _():
+            unit([low], pair, zc, False)
+    def two_heads(tile):
+        tile = jnp.exp(tile)
+        return jnp.concatenate(
+            [jnp.broadcast_to(tile[4 * e : 4 * e + 1], (SSM_P, 128)) for e in range(2)], axis=0
+        )
+
+    def take(t):
+        wait_chunk(6, at[t])
+        if t < 2:
+            to_neighbour(6, at[t], 4, right, 8 + t).start()
+        to_partner(6, at[t]).start()
+        wait_chunk(2, at[t])
+        if t >= 2:
+            to_neighbour(2, at[t], 4, left, 8 + t).start()
+        to_partner(2, at[t]).start()
+
+    take(0)
     for t in range(4):
         arrived(q.at[at[t]], zq_recv.at[at[t]])
-    for t in range(4):
-        over(0, t)
-    for dy in range(1, 4):
-        yy = lax.rem(y + dy, 4)
-        arrived(st_y.at[yy], sty_recv.at[0, yy])
-        arrived(tot_y.at[yy], sty_recv.at[1, yy])
-    row_before, row_total = prefix(st_y, tot_y, y, row_out, rtot_out)
-    state[...] = row_before
-    tot_out2 = row_total
-    for dz in range(1, 4):
-        where = {"sp_0": lax.rem(z + dz, 4)}
-        remote(row_out, st_z.at[z], stz_send.at[0, dz], stz_recv.at[0, z], where).start()
-        remote(rtot_out, tot_z.at[z], stz_send.at[1, dz], stz_recv.at[1, z], where).start()
-    for t in range(4):
-        wait_chunk(1, at[t])
-        over(1, t)
-
-    def finish_ssm():
+
+    def own_chunk(t, carry):
+        zc = jnp.where(t == 0, at[0], jnp.where(t == 1, at[1], jnp.where(t == 2, at[2], at[3])))
+        wait_chunk(1, zc)
+        unit([zc], 0, zc, True)
+        over(0, zc, zc + 1)
+        return carry
+
+    lax.fori_loop(0, 4, own_chunk, 0)
+
+    def row_prefix():
+        for dy in range(1, 4):
+            yy = lax.rem(y + dy, 4)
+            arrived(st_y.at[yy], sty_recv.at[0, yy])
+            arrived(tot_y.at[yy], sty_recv.at[1, yy])
+        run_s, run_t = jnp.zeros((128, 128), F32), jnp.zeros((8, 128), F32)
+        for k in range(4):
+            pre_s[k] = run_s
+            pre_t[k] = run_t
+            run_s = run_s * two_heads(tot_y[k]) + st_y[k].astype(F32)
+            run_t = run_t + tot_y[k]
+        row_out[...] = run_s.astype(BF16)
+        rtot_out[...] = run_t
+        st_z[z] = run_s.astype(BF16)
+        tot_z[z] = run_t
+        for dz in range(1, 4):
+            where = {"sp_0": lax.rem(z + dz, 4)}
+            remote(row_out, st_z.at[z], stz_send.at[0, dz], stz_recv.at[0, z], where).start()
+            remote(rtot_out, tot_z.at[z], stz_send.at[1, dz], stz_recv.at[1, z], where).start()
+
+    def far_prefix():
         for dz in range(1, 4):
             zz = lax.rem(z + dz, 4)
             arrived(st_z.at[zz], stz_recv.at[0, zz])
             arrived(tot_z.at[zz], stz_recv.at[1, zz])
-        far, _ = prefix(st_z, tot_z, z, None, None)
-        state[...] = far * by_head(jnp.exp(tot_out2)) + state[...]
+        run = jnp.zeros((128, 128), F32)
+        for k in range(3):
+            run = jnp.where(k < z, run * two_heads(tot_z[k]) + st_z[k].astype(F32), run)
+        for k in range(4):
+            inc_out[k] = (run * two_heads(pre_t[k]) + pre_s[k]).astype(BF16)
+        inc_in[y] = inc_out[y]
+        for dy in range(1, 4):
+            yy = lax.rem(y + dy, 4)
+            remote(inc_out.at[yy], inc_in.at[y], inc_send.at[yy], inc_recv.at[y], {"sp_1": yy}).start()
+
+    def finish_ssm():
+        for dy in range(1, 4):
+            yy = lax.rem(y + dy, 4)
+            arrived(inc_in.at[yy], inc_recv.at[yy])
+        came = [jnp.concatenate([inc_in[2 * g], inc_in[2 * g + 1]], axis=0) for g in range(2)]
         for n in range(4):
             rows = slice(n * BLOCK, (n + 1) * BLOCK)
             for g in range(2):
                 lanes = slice(g * 256, (g + 1) * 256)
                 inputs_c = act[rows, 768 + g * 128 : 896 + g * 128]
-                value = ysum[rows, lanes] + split_dot(inputs_c, state[lanes, :]) * spread(
+                value = ysum[rows, lanes] + contract(inputs_c, came[g], 1, 1) * spread(
                     cols[rows, :], 24 + 4 * g
                 )
                 opened = gate[rows, lanes].astype(F32)
@@ -494,66 +550,87 @@
                 ssm_buf[1], wo[1, 1, :, lanes]
             )
 
-    for t in range(4):
-        wait_chunk(6, at[t])
-        if t < 2:
-            to_neighbour(6, at[t], 4, right, 8 + t).start()
-        to_partner(6, at[t]).start()
-        wait_chunk(2, at[t])
-        if t >= 2:
-            to_neighbour(2, at[t], 4, left, 8 + t).start()
-        to_partner(2, at[t]).start()
-        over(6, t)
-        over(2, t)
-        if t:
-            wait_chunk(7, at[t - 1])
-            over(7, t - 1)
-            wait_chunk(3, at[t - 1])
-            over(3, t - 1)
-        if t == 0:
-            finish_ssm()
-        if t == 1:
-            project_ssm()
-    wait_chunk(7, at[3])
-    over(7, 3)
-    wait_chunk(3, at[3])
-    over(3, 3)
-    for t in (0, 2, 1, 3):
+    def finish(zq, carry):
+        differ = acc[zq, 0] / total[zq, 0, 0:1] - lam * (acc[zq, 1] / total[zq, 1, 0:1])
+        scale = lax.rsqrt(jnp.mean(differ * differ, axis=0, keepdims=True) + EPS)
+        done_out[zq] = (differ * scale * gain_col[...]).astype(BF16)
+
+        @pl.when(zq == z)
+        def _():
+            pltpu.make_async_copy(done_out.at[zq], back.at[z], back_recv.at[z]).start()
+
+        @pl.when(zq != z)
+        def _():
+            remote(
+                done_out.at[zq], back.at[z], back_send.at[zq], back_recv.at[z], {"sp_0": zq}
+            ).start()
+
+        return carry
+
+    def later(pair, zc):
+        return zc + jnp.where(lax.rem(y + pair, 4) > y, 1, 0)
+
+    def near(t):
+        def side(k, carry):
+            pair = 3 - 2 * k
+            wait_chunk(2 * pair + 1, at[t])
+            over(pair, at[t], later(pair, at[t]))
+            return carry
+
+        lax.fori_loop(0, 2, side, 0)
+
+    def take_far(t):
         wait_chunk(4, at[t])
         to_partner(4, at[t]).start()
-        over(4, t)
-    for t in (0, 2, 1, 3):
+
+    def far(t):
         wait_chunk(5, at[t])
-        over(5, t)
-
+        over(2, at[t], later(2, at[t]))
+
+    row_prefix()
+    take(1)
+    near(0)
+    take(2)
+    far_prefix()
+    near(1)
+    take(3)
+    near(2)
+    take_far(0)
+    near(3)
+    far(0)
+    take_far(1)
+    finish_ssm()
+    project_ssm()
+    take_far(2)
+    far(1)
+    far(2)
     arrived(lam_in, lam_sem.at[1])
     held = jnp.where(z // 2 == c, lam_own[lax.rem(z, 2)], lam_in[lax.rem(z, 2)])
     lam = jnp.concatenate([held, held], axis=1)[0:1]
-    gain_col = jnp.broadcast_to(head_gain[...], (PAIR, PAIR)).T
-    for dz in ORDER:
-        zz = lax.rem(z + dz, 4)
-        differ = acc[zz, 0] / total[zz, 0, 0:1] - lam * (acc[zz, 1] / total[zz, 1, 0:1])
-        scale = lax.rsqrt(jnp.mean(differ * differ, axis=0, keepdims=True) + EPS)
-        done_out[zz] = (differ * scale * gain_col).astype(BF16)
-        if dz == 0:
-            back[zz] = done_out[zz]
-        else:
-            remote(
-                done_out.at[zz], back.at[z], back_send.at[dz], back_recv.at[z], {"sp_0": zz}
-            ).start()
+    gain_col[...] = jnp.broadcast_to(head_gain[...], (PAIR, PAIR)).T
+    lax.fori_loop(0, at[3], finish, 0)
+    take_far(3)
+    far(3)
+    lax.fori_loop(at[3], 4, finish, 0)
+    out_copies = []
     loads[10].wait()
     arrived(wo.at[other, 0], wo_sem.at[3])
-    for dz in range(1, 4):
-        zz = lax.rem(z + dz, 4)
-        arrived(back.at[zz], back_recv.at[zz])
-    for k in range(4):
-        lanes = slice(k * 512, (k + 1) * 512)
-        sum_k = joined[:, lanes]
-        for h in range(4):
-            sum_k = sum_k + contract(
-                back[h], wo[h // 2, 0, (h % 2) * PAIR : (h % 2 + 1) * PAIR, lanes], 0, 0
-            )
-        out_ref[:, lanes] = sum_k.astype(BF16)
+    for k, h in enumerate((z, lax.rem(z + 3, 4), lax.rem(z + 1, 4), lax.rem(z + 2, 4))):
+        arrived(back.at[h], back_recv.at[h])
+        weight = wo.at[h // 2, 0, pl.ds(pl.multiple_of(lax.rem(h, 2) * PAIR, PAIR), PAIR)]
+        for n in range(4):
+            lanes = slice(n * 512, (n + 1) * 512)
+            sum_n = joined[:, lanes] + contract(back[h], weight[:, lanes], 0, 0)
+            if k < 3:
+                joined[:, lanes] = sum_n
+            else:
+                result[:, lanes] = sum_n.astype(BF16)
+                out_copies.append(
+                    pltpu.make_async_copy(
+                        result.at[:, lanes], out_ref.at[:, lanes], out_sem.at[n]
+                    )
+                )
+                out_copies[-1].start()
 
     x_copy.wait_send()
     lam_copy.wait_send()
@@ -574,12 +651,17 @@
         for t in range(4):
             arrived(kv.at[0, 0], core_send.at[s, t])
     for d in range(1, 4):
-        arrived(done_out.at[0], back_send.at[d])
-        arrived(st_out, sty_send.at[0, d])
-        arrived(tot_out, sty_send.at[1, d])
+        yy = lax.rem(y + d, 4)
+        arrived(st_out.at[yy], sty_send.at[0, yy])
+        arrived(tot_out.at[yy], sty_send.at[1, yy])
+        arrived(inc_out.at[yy], inc_send.at[yy])
         arrived(row_out, stz_send.at[0, d])
         arrived(rtot_out, stz_send.at[1, d])
     arrived(ssm_all.at[0], ssm_sem.at[0])
+    for d in range(1, 4):
+        arrived(done_out.at[0], back_send.at[lax.rem(z + d, 4)])
+    for copy in out_copies:
+        copy.wait()
 
 
 def per_device(
@@ -616,7 +698,7 @@
         + [away] * 8
         + [vmem] * 3
         + [smem, vmem, smem, vmem, vmem, away, away],
-        out_specs=vmem,
+        out_specs=away,
         scratch_shapes=[
             buf((2, ROWS, 1024), BF16),
             buf((ROWS, D), BF16),
@@ -627,7 +709,7 @@
             buf((D, 512), BF16),
             buf((D, 256), BF16),
             buf((D, 256), BF16),
-            buf((D, 8), BF16),
+            buf((8, D), BF16),
             buf((2, 2, 512, D), BF16),
             buf((4, 2, HALF, PAIR), BF16),
             buf((4, PAIR, HALF), BF16),
@@ -643,23 +725,29 @@
             buf((16, 1024), BF16),
             buf((ROWS, 1024), BF16),
             buf((ROWS, 512), BF16),
-            buf((2, ROWS, 128), F32),
+            buf((8, ROWS), F32),
             buf((ROWS, 128), F32),
             buf((ROWS, 512), F32),
             buf((512, 128), F32),
-            buf((512, 128), BF16),
+            buf((4, 128, 128), BF16),
+            buf((4, 8, 128), F32),
+            buf((4, 128, 128), BF16),
+            buf((4, 8, 128), F32),
+            buf((128, 128), BF16),
             buf((8, 128), F32),
-            buf((4, 512, 128), BF16),
+            buf((4, 128, 128), BF16),
             buf((4, 8, 128), F32),
-            buf((512, 128), BF16),
-            buf((8, 128), F32),
-            buf((4, 512, 128), BF16),
+            buf((4, 128, 128), F32),
             buf((4, 8, 128), F32),
+            buf((4, 128, 128), BF16),
+            buf((4, 128, 128), BF16),
             buf((2, HALF, 512), BF16),
             buf((2, HALF, 512), BF16),
             buf((HALF, D), F32),
             buf((2, 8, 128), F32),
             buf((2, 8, 128), F32),
+            buf((PAIR, PAIR), F32),
+            buf((HALF, D), BF16),
             dma((11,)),
             dma((2,)),
             dma((4,)),
@@ -679,6 +767,9 @@
             dma((2, 4)),
             dma((2,)),
             dma((2,)),
+            dma((4,)),
+            dma((4,)),
+            dma((4,)),
         ],
         compiler_params=pltpu.CompilerParams(
             collective_id=0, has_side_effects=True, vmem_limit_bytes=63 * 2**20
@@ -693,12 +784,12 @@
         w_inner,
         w_bvec,
         w_cvec,
-        w_step,
+        w_step.T,
         conv_inner,
         conv_bvec,
         conv_cvec,
         a_log.reshape(1, 8),
-        decay_add,
+        decay_add.T,
         lambdas.reshape(1, 2),
         head_gain.reshape(1, PAIR),
         ssm_gain.reshape(1, 512),

time: 98 us -> 80.2 us (0.82)
  the two profiles are of different devices: /device:TPU:31 before, /device:TPU:1 now
where the time goes in v3:
time: 80.2 us; the launch traced here: 80 us
  Pallas kernels  77.7 us (97%)
  local copies, waits for them, and re-layouts  2.3 us (3%)
    pallas_call x1, Pallas kernels, per_device(): pl.pallas_call(layer_kernel, out_shape=jax.ShapeDtypeStruct((HALF, D), BF...  77.7 us
    unnamed x1, local copies, waits for them, and re-layouts  2.3 us

profile of v3, /device:TPU:1, one launch (start us, length us, event | category | flops | bytes accessed | tf_op | source)
XLA Modules:
  0.0 80.0 jit_solution(2378778683533783377)
XLA Ops:
  0.0 77.7 %shard_map.190 = bf16[256,2048]{1,0:T(8,128)(2,1)} custom-call(bf16[512,1024]{1,0:T(8,128)(2,1)} %hidden.1, f32[1,2048]{1,0:T(1,128)} %bitcast.9, bf16[2048,512]{1,0:T(8,128)(2,1)} %w_query.1, bf16[2048,512]{1,0:T(8,128)(2,1)} %w_key.1, bf16[2048,512]{1,0:T(8,128)(2,1)} %w_value.1, bf16[2048,512]{1,0:T(8,128)(2,1)} %w_gate.1, bf16[2048,512]{1,0:T(8,128)(2,1)} %w_inner.1, ...), custom_call_target="tpu_custom_call" | custom-call | tf_op jit(solution)/shard_map/pallas_call | solution.py:694
  77.7 2.3 %copy.22 = bf16[256,2048]{1,0:T(8,128)(2,1)} copy(bf16[256,2048]{1,0:T(8,128)(2,1)} %shard_map.190) | data formatting | bytes 2097152

commit v4 on v3

--- a/solution.py
+++ b/solution.py
@@ -600,16 +600,18 @@
     far(0)
     take_far(1)
     finish_ssm()
-    project_ssm()
     take_far(2)
     far(1)
-    far(2)
     arrived(lam_in, lam_sem.at[1])
     held = jnp.where(z // 2 == c, lam_own[lax.rem(z, 2)], lam_in[lax.rem(z, 2)])
     lam = jnp.concatenate([held, held], axis=1)[0:1]
     gain_col[...] = jnp.broadcast_to(head_gain[...], (PAIR, PAIR)).T
-    lax.fori_loop(0, at[3], finish, 0)
+    whole = jnp.where(z < 2, 2, z - 2)
+    lax.fori_loop(0, whole, finish, 0)
+    project_ssm()
     take_far(3)
+    far(2)
+    lax.fori_loop(whole, at[3], finish, 0)
     far(3)
     lax.fori_loop(at[3], 4, finish, 0)
     out_copies = []

time: 80.2 us -> 77.1 us (0.961)
  Pallas kernels: 77.7 us -> 74.6 us
    pallas_call x1, Pallas kernels: 77.7 us -> 74.6 us  [per_device(): pl.pallas_call(layer_kernel, out_shape=jax.ShapeDtypeStruct((HALF, D), BF...]
where the time goes in v4:
time: 77.1 us; the launch traced here: 76.9 us
  Pallas kernels  74.6 us (97%)
  local copies, waits for them, and re-layouts  2.3 us (3%)
    pallas_call x1, Pallas kernels, per_device(): pl.pallas_call(layer_kernel, out_shape=jax.ShapeDtypeStruct((HALF, D), BF...  74.6 us
    unnamed x1, local copies, waits for them, and re-layouts  2.3 us

profile of v4, /device:TPU:1, one launch (start us, length us, event | category | flops | bytes accessed | tf_op | source)
XLA Modules:
  0.0 76.9 jit_solution(12151948414063826119)
XLA Ops:
  0.0 74.6 %shard_map.190 = bf16[256,2048]{1,0:T(8,128)(2,1)} custom-call(bf16[512,1024]{1,0:T(8,128)(2,1)} %hidden.1, f32[1,2048]{1,0:T(1,128)} %bitcast.9, bf16[2048,512]{1,0:T(8,128)(2,1)} %w_query.1, bf16[2048,512]{1,0:T(8,128)(2,1)} %w_key.1, bf16[2048,512]{1,0:T(8,128)(2,1)} %w_value.1, bf16[2048,512]{1,0:T(8,128)(2,1)} %w_gate.1, bf16[2048,512]{1,0:T(8,128)(2,1)} %w_inner.1, ...), custom_call_target="tpu_custom_call" | custom-call | tf_op jit(solution)/shard_map/pallas_call | solution.py:696
  74.6 2.3 %copy.22 = bf16[256,2048]{1,0:T(8,128)(2,1)} copy(bf16[256,2048]{1,0:T(8,128)(2,1)} %shard_map.190) | data formatting | bytes 2097152

commit v5 on v4

--- a/solution.py
+++ b/solution.py
@@ -471,13 +471,19 @@
         to_partner(2, at[t]).start()
 
     take(0)
-    for t in range(4):
+    arrived(q.at[z], zq_recv.at[z])
+    wait_chunk(1, z)
+    unit([z], 0, z, True)
+    for t in range(1, 4):
         arrived(q.at[at[t]], zq_recv.at[at[t]])
 
     def own_chunk(t, carry):
         zc = jnp.where(t == 0, at[0], jnp.where(t == 1, at[1], jnp.where(t == 2, at[2], at[3])))
-        wait_chunk(1, zc)
-        unit([zc], 0, zc, True)
+        @pl.when(t > 0)
+        def _():
+            wait_chunk(1, zc)
+            unit([zc], 0, zc, True)
+
         over(0, zc, zc + 1)
         return carry
 
@@ -608,10 +614,10 @@
     gain_col[...] = jnp.broadcast_to(head_gain[...], (PAIR, PAIR)).T
     whole = jnp.where(z < 2, 2, z - 2)
     lax.fori_loop(0, whole, finish, 0)
+    far(2)
+    take_far(3)
+    lax.fori_loop(whole, at[3], finish, 0)
     project_ssm()
-    take_far(3)
-    far(2)
-    lax.fori_loop(whole, at[3], finish, 0)
     far(3)
     lax.fori_loop(at[3], 4, finish, 0)
     out_copies = []

time: 77.1 us -> 77.1 us (level)
  no operation moved by 1% of the time
where the time goes in v5:
time: 77.1 us; the launch traced here: 76.9 us
  Pallas kernels  74.6 us (97%)
  local copies, waits for them, and re-layouts  2.3 us (3%)
    pallas_call x1, Pallas kernels, per_device(): pl.pallas_call(layer_kernel, out_shape=jax.ShapeDtypeStruct((HALF, D), BF...  74.6 us
    unnamed x1, local copies, waits for them, and re-layouts  2.3 us

profile of v5, /device:TPU:1, one launch (start us, length us, event | category | flops | bytes accessed | tf_op | source)
XLA Modules:
  0.0 76.9 jit_solution(9777105173919632548)
XLA Ops:
  0.0 74.6 %shard_map.190 = bf16[256,2048]{1,0:T(8,128)(2,1)} custom-call(bf16[512,1024]{1,0:T(8,128)(2,1)} %hidden.1, f32[1,2048]{1,0:T(1,128)} %bitcast.9, bf16[2048,512]{1,0:T(8,128)(2,1)} %w_query.1, bf16[2048,512]{1,0:T(8,128)(2,1)} %w_key.1, bf16[2048,512]{1,0:T(8,128)(2,1)} %w_value.1, bf16[2048,512]{1,0:T(8,128)(2,1)} %w_gate.1, bf16[2048,512]{1,0:T(8,128)(2,1)} %w_inner.1, ...), custom_call_target="tpu_custom_call" | custom-call | tf_op jit(solution)/shard_map/pallas_call | solution.py:702
  74.6 2.3 %copy.22 = bf16[256,2048]{1,0:T(8,128)(2,1)} copy(bf16[256,2048]{1,0:T(8,128)(2,1)} %shard_map.190) | data formatting | bytes 2097152
